TPU v7x, 256 devices: a whole 4x4x8 slice. The times are simulated.
256 devices in a mesh: dp: 4 (over y), kv: 32 (over z, x), tp: 2 (over core).
Axes of the slice: x: 4, y: 4, z: 8, core: 2. Of those that a mesh axis runs over, the one named last changes fastest.
Arguments:
- tokens: bfloat16 [2048, 2048], P('dp', ('kv', 'tp')), parts along dimension 0, may hold values from -64 to 64, as said below
- lengths: int32 [256], P(('dp', 'kv', 'tp')), parts along dimension 0, may hold values from 1 to 8, 224 in all
- state: float32 [256, 16, 128, 128], P(('dp', 'kv', 'tp')), parts along dimension 0, may hold values from -1.8 to 1.8
- gain_first: float32 [2048], replicated, may hold values from 0.1 to 1.9
- first_gate: bfloat16 [2048, 5632], P(None, 'kv'), may hold values from -0.125 to 0.125
- first_up: bfloat16 [2048, 5632], P(None, 'kv'), may hold values from -0.125 to 0.125
- first_down: bfloat16 [5632, 2048], P('kv'), may hold values from -0.15625 to 0.15625
- gain_mix: float32 [2048], replicated, may hold values from 0.1 to 1.9
- query_weight: bfloat16 [2048, 2048], P(None, ('kv', 'tp')), may hold values from -0.125 to 0.125
- key_weight: bfloat16 [2048, 2048], P(None, ('kv', 'tp')), may hold values from -0.125 to 0.125
- value_weight: bfloat16 [2048, 2048], P(None, ('kv', 'tp')), may hold values from -0.125 to 0.125
- gating_weight: bfloat16 [2048, 2048], P(None, ('kv', 'tp')), may hold values from -0.125 to 0.125
- write_weight: bfloat16 [2048, 16], replicated, may hold values from -0.125 to 0.125
- forget_weight: bfloat16 [2048, 16], replicated, may hold values from -0.125 to 0.125
- forget_rate: float32 [16], replicated, may hold values from -4 to 1.5
- out_weight: bfloat16 [2048, 2048], P(None, ('kv', 'tp')), may hold values from -0.125 to 0.125
- gain_second: float32 [2048], replicated, may hold values from 0.1 to 1.9
- second_gate: bfloat16 [2048, 5632], P(None, 'kv'), may hold values from -0.125 to 0.125
- second_up: bfloat16 [2048, 5632], P(None, 'kv'), may hold values from -0.125 to 0.125
- second_down: bfloat16 [5632, 2048], P('kv'), may hold values from -0.15625 to 0.15625
Outputs:
- mixed_out: bfloat16 [2048, 2048], P('dp', ('kv', 'tp')), parts along dimension 0
- new_state: float32 [256, 16, 128, 128], P(('dp', 'kv', 'tp')), parts along dimension 0
There are 4 independent parts, one for each index of `dp`. A program takes and returns all parts, laid end to end along the dimension named above; an argument that names none is the same for every part. Nothing has to cross between parts.
Inputs may be any that keep to these rules, and one draw needn't show every extreme that they name: Activations of the new tokens. `lengths`: the live new tokens of each sequence; within each independent group of 64 sequences (one part along dp) they sum to seven halves of 64, rounded down, and some sequence of each group has all 8 live.
All inputs are finite; a program needn't handle non-finite values.
Results may differ from a plain program's by a relative error of at most 0.0058.
Values may be sent and summed in bfloat16 or wider, within the bound.
A program may use at most 64 MiB of HBM per device.

v0:
```python
import math

import jax
import jax.numpy as jnp
from jax import lax
from jax.sharding import PartitionSpec as P

HEADS = 16
HEAD = 128
BLK = 8


EPSILON = 1e-06


def laid_out(parts, dim):
    parts = jnp.moveaxis(parts, 0, dim)
    dims = parts.shape
    return parts.reshape(*dims[:dim], dims[dim] * dims[dim + 1], *dims[dim + 2 :])


def copy_for_each(array, axis):
    copies = jnp.broadcast_to(array, (lax.axis_size(axis), *array.shape))
    return lax.all_to_all(copies, axis, split_axis=0, concat_axis=0, tiled=True)


def collect(array, axis, dim):
    return laid_out(copy_for_each(array, axis), dim)


def cut_along(array, dim, count):
    before, after = (array.shape[:dim], array.shape[dim + 1 :])
    return jnp.moveaxis(array.reshape(*before, count, -1, *after), dim, 0)


def sum_at_owner(array, axis, dim):
    parts = cut_along(array, dim, lax.axis_size(axis))
    arrived = lax.all_to_all(parts, axis, split_axis=0, concat_axis=0, tiled=True)
    return arrived.astype(jnp.float32).sum(axis=0)


def fold_step(gain, gate_cols, up_cols, portion):
    values = portion.astype(jnp.float32)
    scaled = (values * gain).astype(jnp.bfloat16)
    gate_acc = jnp.dot(scaled, gate_cols, preferred_element_type=jnp.float32)
    up_acc = jnp.dot(scaled, up_cols, preferred_element_type=jnp.float32)
    squares = jnp.sum(values * values, axis=1)
    return (gate_acc, up_acc, squares)


def finish_units(gate_acc, up_acc, squares, channels, down_rows):
    row_scale = lax.rsqrt(squares / channels + EPSILON)[:, None]
    hidden = (jax.nn.silu(gate_acc * row_scale) * (up_acc * row_scale)).astype(jnp.bfloat16)
    return jnp.dot(hidden, down_rows, preferred_element_type=jnp.float32)


def feed_forward(hidden_in, gain, w_gate, w_up, w_down):
    channels = gain.shape[0]
    paired = lax.all_to_all(hidden_in, "tp", split_axis=0, concat_axis=1, tiled=True)
    gate_acc, up_acc, squares = fold_step(gain, w_gate, w_up, collect(paired, "kv", 1))
    ffn_term = finish_units(gate_acc, up_acc, squares, channels, w_down)
    partial_value = sum_at_owner(ffn_term.astype(jnp.bfloat16), "kv", 1)
    summed = lax.all_to_all(partial_value, "tp", split_axis=1, concat_axis=0, tiled=True)
    return (hidden_in.astype(jnp.float32) + 0.5 * summed).astype(jnp.bfloat16)


def delta_block(query, key_in, value, gating, write_pre, forget_pre, rates, live, state):
    seq_count, block_len, head_count, head_size = query.shape
    precise = lax.Precision.HIGHEST
    query_unit = (
        query
        * lax.rsqrt(jnp.sum(query * query, axis=-1, keepdims=True) + EPSILON)
        / math.sqrt(head_size)
    )
    key_unit = key_in * lax.rsqrt(jnp.sum(key_in * key_in, axis=-1, keepdims=True) + EPSILON)
    live_rows = live[:, :, None]
    write_gate = jax.nn.sigmoid(write_pre) * live_rows
    forget = -jnp.exp(rates)[None, None, :] * jax.nn.softplus(forget_pre) * live_rows
    cumulative = jnp.cumsum(forget, axis=1)
    cum_heads = jnp.transpose(cumulative, (0, 2, 1))
    positions = jnp.arange(block_len)
    causal = positions[:, None] >= positions[None, :]
    strict = positions[:, None] > positions[None, :]
    differ = jnp.minimum(cum_heads[:, :, :, None] - cum_heads[:, :, None, :], 0.0)
    decay_mat = jnp.where(causal, jnp.exp(differ), 0.0)
    key_dots = jnp.einsum("sthd,suhd->shtu", key_unit, key_unit, precision=precise)
    write_heads = jnp.transpose(write_gate, (0, 2, 1))
    strict_part = jnp.where(strict, write_heads[:, :, :, None] * decay_mat * key_dots, 0.0)
    identity = jnp.eye(block_len, dtype=jnp.float32)
    squared = jnp.einsum("shtu,shuv->shtv", strict_part, strict_part, precision=precise)
    fourth = jnp.einsum("shtu,shuv->shtv", squared, squared, precision=precise)
    inverse = jnp.einsum(
        "shtu,shuv->shtv", identity - strict_part, identity + squared, precision=precise
    )
    inverse = jnp.einsum("shtu,shuv->shtv", inverse, identity + fourth, precision=precise)
    growth = jnp.exp(cumulative)
    target = jnp.einsum(
        "shtu,suhv->sthv", inverse, write_gate[..., None] * value, precision=precise
    )
    key_mix = jnp.einsum(
        "shtu,suhk->sthk", inverse, (write_gate * growth)[..., None] * key_unit, precision=precise
    )
    update = target - jnp.einsum("sthk,shkv->sthv", key_mix, state, precision=precise)
    scores = jnp.einsum("sthd,suhd->shtu", query_unit, key_unit, precision=precise) * decay_mat
    attend = jnp.einsum("sthk,shkv->sthv", query_unit * growth[..., None], state, precision=precise)
    attend = attend + jnp.einsum("shtu,suhv->sthv", scores, update, precision=precise)
    final_cum = cumulative[:, -1:, :]
    fading = jnp.exp(final_cum - cumulative)
    new_state = jnp.exp(final_cum[:, 0, :])[:, :, None, None] * state
    new_state = new_state + jnp.einsum(
        "sthk,sthv->shkv", key_unit * fading[..., None], update, precision=precise
    )
    normed = attend * lax.rsqrt(jnp.mean(attend * attend, axis=-1, keepdims=True) + EPSILON)
    normed = normed * jax.nn.silu(gating) * live[:, :, None, None]
    mixed_heads = normed.reshape(seq_count * block_len, head_count * head_size).astype(jnp.bfloat16)
    return (mixed_heads, new_state)


def per_device(
    tokens,
    lengths,
    state,
    gain_first,
    first_gate,
    first_up,
    first_down,
    gain_mix,
    query_weight,
    key_weight,
    value_weight,
    gating_weight,
    write_weight,
    forget_weight,
    forget_rate,
    out_weight,
    gain_second,
    second_gate,
    second_up,
    second_down,
):
    after_first = feed_forward(tokens, gain_first, first_gate, first_up, first_down)
    seq_count = lengths.shape[0]
    own_count = seq_count * BLK
    whole_rows = collect(after_first, ("kv", "tp"), 1)
    scaled_all = (whole_rows.astype(jnp.float32) * gain_mix).astype(jnp.bfloat16)
    stacked = jnp.stack(
        [
            jnp.dot(scaled_all, matrix, preferred_element_type=jnp.float32)
            for matrix in (query_weight, key_weight, value_weight, gating_weight)
        ]
    )
    owned = lax.all_to_all(
        stacked.astype(jnp.bfloat16), ("kv", "tp"), split_axis=1, concat_axis=2, tiled=True
    ).astype(stacked.dtype)
    row_start = lax.axis_index(("kv", "tp")) * own_count
    own_values = lax.dynamic_slice_in_dim(whole_rows, row_start, own_count, 0).astype(jnp.float32)
    own_scaled = lax.dynamic_slice_in_dim(scaled_all, row_start, own_count, 0)
    mix_scale = lax.rsqrt(jnp.mean(own_values * own_values, axis=1, keepdims=True) + EPSILON)
    query = (owned[0] * mix_scale).reshape(seq_count, BLK, HEADS, HEAD)
    key_in = (owned[1] * mix_scale).reshape(seq_count, BLK, HEADS, HEAD)
    value = (owned[2] * mix_scale).reshape(seq_count, BLK, HEADS, HEAD)
    gating = (owned[3] * mix_scale).reshape(seq_count, BLK, HEADS, HEAD)
    write_pre = (
        jnp.dot(own_scaled, write_weight, preferred_element_type=jnp.float32) * mix_scale
    ).reshape(seq_count, BLK, HEADS)
    forget_pre = (
        jnp.dot(own_scaled, forget_weight, preferred_element_type=jnp.float32) * mix_scale
    ).reshape(seq_count, BLK, HEADS)
    positions = jnp.arange(BLK, dtype=jnp.int32)
    live = (positions[None, :] < lengths[:, None]).astype(jnp.float32)
    mixed_heads, new_state = delta_block(
        query, key_in, value, gating, write_pre, forget_pre, forget_rate, live, state
    )
    half_cols = mixed_heads.shape[1] // 2
    portion = collect(mixed_heads, ("kv", "tp"), 0)
    first_half = jnp.dot(
        portion[:, :half_cols], out_weight[:half_cols], preferred_element_type=jnp.float32
    ).astype(jnp.bfloat16)
    second_half = jnp.dot(
        portion[:, half_cols:], out_weight[half_cols:], preferred_element_type=jnp.float32
    ).astype(jnp.bfloat16)
    first_half, second_half = lax.optimization_barrier((first_half, second_half))
    mixed_sum = first_half.astype(jnp.float32) + second_half.astype(jnp.float32)
    after_mix = (after_first.astype(jnp.float32) + mixed_sum).astype(jnp.bfloat16)
    mixed_out = feed_forward(after_mix, gain_second, second_gate, second_up, second_down)
    return (mixed_out, new_state)


def solution(mesh):
    in_specs = (
        P("dp", ("kv", "tp")),
        P(("dp", "kv", "tp")),
        P(("dp", "kv", "tp"), None, None, None),
        P(),
        P(None, "kv"),
        P(None, "kv"),
        P("kv", None),
        P(),
        P(None, ("kv", "tp")),
        P(None, ("kv", "tp")),
        P(None, ("kv", "tp")),
        P(None, ("kv", "tp")),
        P(),
        P(),
        P(),
        P(None, ("kv", "tp")),
        P(),
        P(None, "kv"),
        P(None, "kv"),
        P("kv", None),
    )
    out_specs = (P("dp", ("kv", "tp")), P(("dp", "kv", "tp"), None, None, None))
    return jax.shard_map(
        per_device, mesh=mesh, in_specs=in_specs, out_specs=out_specs, check_vma=False
    )
```

profile of v0, /device:TPU:1, one launch (start us, length us, event | category | flops | bytes accessed | tf_op | source)
XLA Modules:
  0.0 314.3 jit_solution(10236440952969772282)
XLA Ops:
  0.6 0.8 copy.214
  1.5 6.6 %all_to_all.103 = bf16[2,256,32]{1,2,0:T(8,128)(2,1)S(1)} all-to-all(bf16[2,256,32]{1,2,0:T(8,128)(2,1)S(1)} %bitcast.179), channel_id=1, replica_groups=mesh['dp'=4,'kv'=32,'tp'=2] {'tp'}, dimensions={0} | all-to-all | bytes 65536 | tf_op jit(solution)/shard_map/all_to_all | solution.py:59
  8.2 35.9 %all_to_all.104 = bf16[32,256,64]{1,2,0:T(8,128)(2,1)S(1)} all-to-all(bf16[32,256,64]{1,2,0:T(8,128)(2,1)S(1)} %broadcast_in_dim.16), channel_id=1, replica_groups=mesh['dp'=4,'kv'=32,'tp'=2] {'kv'}, dimensions={0} | all-to-all | bytes 2097152 | tf_op jit(solution)/shard_map/all_to_all | solution.py:24
  44.0 0.3 multiply_reduce_fusion.1
  44.4 0.3 fusion.1
  44.7 0.4 copy-done.3
  45.1 0.4 convolution_multiply_fusion.3
  45.5 2.3 convolution_convert_fusion.1
  47.8 0.5 copy.146
  48.4 31.3 %all_to_all.105 = bf16[32,256,64]{1,2,0:T(8,128)(2,1)S(1)} all-to-all(bf16[32,256,64]{1,2,0:T(8,128)(2,1)S(1)} %bitcast.167), channel_id=1, replica_groups=mesh['dp'=4,'kv'=32,'tp'=2] {'kv'}, dimensions={0} | all-to-all | bytes 2097152 | tf_op jit(solution)/shard_map/all_to_all | solution.py:38
  79.8 6.9 %all_to_all.106 = f32[256,2,32]{0,2,1:T(8,128)S(1)} all-to-all(f32[256,2,32]{0,2,1:T(8,128)S(1)} %bitcast.173), channel_id=1, replica_groups=mesh['dp'=4,'kv'=32,'tp'=2] {'tp'}, dimensions={1} | all-to-all | bytes 131072 | tf_op jit(solution)/shard_map/all_to_all | solution.py:63
  86.7 1.6 broadcast_in_dim.17
  88.3 6.2 %all-to-all-start.4 = ((bf16[64,512,32]{1,2,0:T(8,128)(2,1)}), bf16[64,512,32]{1,2,0:T(8,128)(2,1)S(1)}, u32[]{:S(2)}, u32[]{:S(2)}) async-start(bf16[64,512,32]{1,2,0:T(8,128)(2,1)} %broadcast_in_dim.17), calls=%async_computation.4 | async-start | bytes 4194304 | tf_op jit(solution)/shard_map/all_to_all | solution.py:24
  95.3 49.0 %all-to-all-done.4 = bf16[64,512,32]{1,2,0:T(8,128)(2,1)S(1)} async-done(((bf16[64,512,32]{1,2,0:T(8,128)(2,1)}), bf16[64,512,32]{1,2,0:T(8,128)(2,1)S(1)}, u32[]{:S(2)}, u32[]{:S(2)}) %all-to-all-start.4) | async-done | bytes 2097184 | tf_op jit(solution)/shard_map/all_to_all | solution.py:24
  144.3 0.4 multiply_reduce_fusion.2
  144.6 1.0 copy-done.1
  145.6 2.1 multiply_convert_fusion
  147.7 0.5 fusion.14
  148.2 0.4 copy-done.6
  148.6 0.4 fusion.13
  149.1 0.5 fusion.12
  149.6 0.5 fusion.11
  150.1 0.3 copy.148
  150.4 1.1 reshape.443
  151.5 7.0 %all-to-all-start.5 = ((bf16[64,2,512]{2,1,0:T(2,128)(2,1)}), bf16[64,2,512]{2,1,0:T(2,128)(2,1)S(1)}, u32[]{:S(2)}, u32[]{:S(2)}) async-start(bf16[64,2,512]{2,1,0:T(2,128)(2,1)} %reshape.443), calls=%async_computation.5 | async-start | bytes 262144 | tf_op jit(solution)/shard_map/all_to_all | solution.py:152
  158.4 1.4 fusion.63
  160.0 1.3 fusion.68
  161.4 8.1 %all-to-all-done.5 = bf16[64,2,512]{2,1,0:T(2,128)(2,1)S(1)} async-done(((bf16[64,2,512]{2,1,0:T(2,128)(2,1)}), bf16[64,2,512]{2,1,0:T(2,128)(2,1)S(1)}, u32[]{:S(2)}, u32[]{:S(2)}) %all-to-all-start.5) | async-done | bytes 131104 | tf_op jit(solution)/shard_map/all_to_all | solution.py:152
  169.8 0.3 copy.149
  174.0 1.0 convolution_bitcast_fusion.3
  175.0 1.0 fusion.9
  176.0 0.3 multiply_reduce_fusion.3
  176.9 53.6 %all_to_all.107 = bf16[64,8,2048]{2,1,0:T(8,128)(2,1)S(1)} all-to-all(bf16[64,8,2048]{2,1,0:T(8,128)(2,1)S(1)} %broadcast_in_dim.22), channel_id=1, replica_groups=mesh['dp'=4,'kv'=32,'tp'=2] {'kv','tp'}, dimensions={0} | all-to-all | bytes 4194304 | tf_op jit(solution)/shard_map/all_to_all | solution.py:24
  230.5 0.4 convolution_convert_fusion.7
  230.9 0.4 convolution_convert_fusion.6
  231.4 5.5 %all_to_all.108 = bf16[2,256,32]{1,2,0:T(8,128)(2,1)S(1)} all-to-all(bf16[2,256,32]{1,2,0:T(8,128)(2,1)S(1)} %bitcast.180), channel_id=1, replica_groups=mesh['dp'=4,'kv'=32,'tp'=2] {'tp'}, dimensions={0} | all-to-all | bytes 65536 | tf_op jit(solution)/shard_map/all_to_all | solution.py:59
  237.0 31.0 %all_to_all.109 = bf16[32,256,64]{1,2,0:T(8,128)(2,1)S(1)} all-to-all(bf16[32,256,64]{1,2,0:T(8,128)(2,1)S(1)} %broadcast_in_dim.23), channel_id=1, replica_groups=mesh['dp'=4,'kv'=32,'tp'=2] {'kv'}, dimensions={0} | all-to-all | bytes 2097152 | tf_op jit(solution)/shard_map/all_to_all | solution.py:24
  268.0 0.3 multiply_reduce_fusion
  268.3 0.3 fusion
  268.6 0.4 copy-done.4
  269.1 0.4 convolution_multiply_fusion.1
  269.4 3.5 %convolution_convert_fusion = bf16[256,2048]{1,0:T(8,128)(2,1)} fusion(bf16[176,2048]{1,0:T(8,128)(2,1)} %param.39, bf16[2048,176]{0,1:T(8,128)(2,1)} %param.38, bf16[256,2048]{0,1:T(8,128)(2,1)S(1)} %fusion, f32[256,176]{0,1:T(8,128)S(1)} %convolution_multiply_fusion.1, f32[256]{0:T(256)S(1)} %add_rsqrt_fusion.3), kind=kOutput, calls=%fused_computation.1 | convolution fusion | flops 369938432 | bytes 3720192 | tf_op jit(solution)/shard_map/dot_general | solution.py:54
  272.9 2.3 copy.175
  275.2 5.9 %all-to-all-start.9 = ((bf16[32,256,64]{1,2,0:T(8,128)(2,1)}), bf16[32,256,64]{1,2,0:T(8,128)(2,1)S(1)}, u32[]{:S(2)}, u32[]{:S(2)}) async-start(bf16[32,256,64]{1,2,0:T(8,128)(2,1)} %bitcast.165), calls=%async_computation.9 | async-start | bytes 2097152 | tf_op jit(solution)/shard_map/all_to_all | solution.py:38
  281.1 2.8 fusion.2
  284.0 22.6 %all-to-all-done.9 = bf16[32,256,64]{1,2,0:T(8,128)(2,1)S(1)} async-done(((bf16[32,256,64]{1,2,0:T(8,128)(2,1)}), bf16[32,256,64]{1,2,0:T(8,128)(2,1)S(1)}, u32[]{:S(2)}, u32[]{:S(2)}) %all-to-all-start.9) | async-done | bytes 1048608 | tf_op jit(solution)/shard_map/all_to_all | solution.py:38
  306.8 6.9 %all_to_all.110 = f32[256,2,32]{0,2,1:T(8,128)S(1)} all-to-all(f32[256,2,32]{0,2,1:T(8,128)S(1)} %bitcast.174), channel_id=1, replica_groups=mesh['dp'=4,'kv'=32,'tp'=2] {'tp'}, dimensions={1} | all-to-all | bytes 131072 | tf_op jit(solution)/shard_map/all_to_all | solution.py:63
  313.7 0.6 add_convert_fusion
  (82 shorter events, 5.4 us)
Async XLA Ops:
  0.6 44.9 %copy-start = (bf16[176,2048]{1,0:T(8,128)(2,1)S(1)}, bf16[176,2048]{1,0:T(8,128)(2,1)}, u32[]{:S(2)}) copy-start(bf16[176,2048]{1,0:T(8,128)(2,1)} %param.26) | copy-start | bytes 2162692
  8.1 36.3 %copy-start.10 = (f32[2048]{0:T(1024)S(1)}, f32[2048]{0:T(1024)}, u32[]{:S(2)}) copy-start(f32[2048]{0:T(1024)} %param.23) | copy-start | bytes 24580
  44.0 1.1 copy-start.3
  48.3 38.4 %copy-start.9 = (bf16[512,32]{0,1:T(8,128)(2,1)S(1)}, bf16[512,32]{0,1:T(8,128)(2,1)}, u32[]{:S(2)}) copy-start(bf16[512,32]{0,1:T(8,128)(2,1)} %param.20) | copy-start | bytes 98308
  88.3 6.9 %copy-start.14 = (f32[16]{0:T(128)S(1)}, f32[16]{0:T(128)}, u32[]{:S(2)}) copy-start(f32[16]{0:T(128)} %param.34) | copy-start | bytes 196
  88.3 57.3 %copy-start.11 = (f32[2048]{0:T(1024)S(1)}, f32[2048]{0:T(1024)}, u32[]{:S(2)}) copy-start(f32[2048]{0:T(1024)} %param.27) | copy-start | bytes 24580
  88.3 55.9 %all-to-all-start.4 = ((bf16[64,512,32]{1,2,0:T(8,128)(2,1)}), bf16[64,512,32]{1,2,0:T(8,128)(2,1)S(1)}, u32[]{:S(2)}, u32[]{:S(2)}) async-start(bf16[64,512,32]{1,2,0:T(8,128)(2,1)} %broadcast_in_dim.17), calls=%async_computation.4 | async-start | bytes 4194304 | tf_op jit(solution)/shard_map/all_to_all | solution.py:24
  144.3 1.3 copy-start.1
  145.6 2.1 copy-start.5
  147.7 0.9 copy-start.6
  147.7 1.3 copy-start.7
  148.6 0.9 copy-start.8
  151.5 18.1 %all-to-all-start.5 = ((bf16[64,2,512]{2,1,0:T(2,128)(2,1)}), bf16[64,2,512]{2,1,0:T(2,128)(2,1)S(1)}, u32[]{:S(2)}, u32[]{:S(2)}) async-start(bf16[64,2,512]{2,1,0:T(2,128)(2,1)} %reshape.443), calls=%async_computation.5 | async-start | bytes 262144 | tf_op jit(solution)/shard_map/all_to_all | solution.py:152
  171.0 3.0 copy-start.2
  176.9 53.7 %copy-start.13 = (bf16[2048,32]{0,1:T(8,128)(2,1)S(1)}, bf16[2048,32]{0,1:T(8,128)(2,1)}, u32[]{:S(2)}) copy-start(bf16[2048,32]{0,1:T(8,128)(2,1)} %param.35) | copy-start | bytes 393220
  236.9 31.4 %copy-start.12 = (f32[2048]{0:T(1024)S(1)}, f32[2048]{0:T(1024)}, u32[]{:S(2)}) copy-start(f32[2048]{0:T(1024)} %param.36) | copy-start | bytes 24580
  268.0 1.1 copy-start.4
  275.2 31.4 %all-to-all-start.9 = ((bf16[32,256,64]{1,2,0:T(8,128)(2,1)}), bf16[32,256,64]{1,2,0:T(8,128)(2,1)S(1)}, u32[]{:S(2)}, u32[]{:S(2)}) async-start(bf16[32,256,64]{1,2,0:T(8,128)(2,1)} %bitcast.165), calls=%async_computation.9 | async-start | bytes 2097152 | tf_op jit(solution)/shard_map/all_to_all | solution.py:38
where the time goes:
time: 315 us; the launch traced here: 314 us
  blocking collectives  178 us (57%)
  waiting for transfers between devices  79.8 us (25%)
  starting transfers between devices  19.1 us (6%)
  matrix products  19 us (6%)
  local copies, waits for them, and re-layouts  11.6 us (4%)
  other arithmetic  5.37 us (2%)
    all_to_all x3, blocking collectives, copy_for_each(): return lax.all_to_all(copies, axis, split_axis=0, concat_axis=0, tiled=True)  120 us
    all_to_all x1, waiting for transfers between devices, copy_for_each(): return lax.all_to_all(copies, axis, split_axis=0, concat_axis=0, tiled=True)  49 us
    all_to_all x1, blocking collectives, sum_at_owner(): lax.all_to_all(parts, axis, split_axis=0, concat_axis=0, tiled=True)  31.3 us
    all_to_all x1, waiting for transfers between devices, sum_at_owner(): lax.all_to_all(parts, axis, split_axis=0, concat_axis=0, tiled=True)  22.6 us
    all_to_all x2, blocking collectives, feed_forward(): lax.all_to_all(partial_value, 'tp', split_axis=1, concat_axis=0, tiled=True)  13.8 us
    all_to_all x2, blocking collectives, feed_forward(): lax.all_to_all(hidden_in, 'tp', split_axis=0, concat_axis=1, tiled=True)  12.1 us
    all_to_all x1, waiting for transfers between devices, per_device(): lax.all_to_all(stacked.astype(jnp.bfloat16), ('kv', 'tp'), split_axis=1,...  8.14 us
    all_to_all x1, starting transfers between devices, per_device(): lax.all_to_all(stacked.astype(jnp.bfloat16), ('kv', 'tp'), split_axis=1,...  6.97 us
  transfers between devices with their start and end apart: 3, of which 3 were waited for; matrix products, arithmetic and copies ran while one was open for 2% of the time, Pallas kernels for 0%

commit v1 on v0

v1 whole, which is shorter than its diff:
```python
import math

import jax
import jax.numpy as jnp
from jax import lax
from jax.experimental import pallas as pl
from jax.experimental.pallas import tpu as pltpu
from jax.sharding import PartitionSpec as P

HEADS = 16
HEAD = 128
BLK = 8
D = 2048
NX = 4
NZ = 8
CHIPS = NX * NZ
ROWS = CHIPS * BLK
EPSILON = 1e-06
F32 = jnp.float32
BF16 = jnp.bfloat16
HIGH = lax.Precision.HIGHEST
DZ_FAR = (4, 3, -3, 2, -2, 1, -1, 0)


def lanes_swapped(tiles):
    rows = tiles[0].shape[0]
    lane = lax.broadcasted_iota(jnp.int32, (rows, 128), 1)
    out = list(tiles)
    for step in (2, 1):
        width = step * 32
        low = (lane & width) == 0
        for i in range(4):
            if i & step:
                continue
            a, b = out[i], out[i + step]
            out[i] = jnp.where(low, a, pltpu.roll(b, width, 1))
            out[i + step] = jnp.where(low, pltpu.roll(a, 128 - width, 1), b)
    return out


def wrapped(dz):
    return (dz + 3) % NZ - 3


def place(dx, dz):
    return (dx % NX) * NZ + dz % NZ


def children(half, dx, dz):
    sign = 1 if half == 0 else -1
    dx, dz = dx % NX, wrapped(dz)
    found = []
    if dx == 0:
        if dz == 0:
            found += [(0, sign * 2), (0, -sign * 3), (0, sign * 3), (0, -sign * 2), (0, 1), (0, -1)]
        if dz == sign * 2:
            found.append((0, 4))
        found += [(1, dz), (-1, dz)]
    elif dx == sign % NX:
        found.append((2, dz))
    return found


ARRIVALS = (
    [(0, 1), (0, -1), (1, 0), (-1, 0), (0, 2), (0, -2)]
    + [(1, 1), (-1, 1), (1, -1), (-1, -1), (0, 3), (0, -3)]
    + [(1, 2), (-1, 2), (1, -2), (-1, -2), (0, 4)]
    + [(1, 3), (-1, 3), (1, -3), (-1, -3), (2, 0), (2, 1), (2, -1)]
    + [(1, 4), (-1, 4), (2, 2), (2, -2), (2, 3), (2, -3), (2, 4)]
)


class Torus:
    def __init__(self):
        self.kv = lax.axis_index("kv")
        self.tp = lax.axis_index("tp")
        self.x = lax.rem(self.kv, NX)
        self.z = lax.div(self.kv, NX)

    def at(self, dx, dz):
        return lax.rem(self.z + dz % NZ, NZ) * NX + lax.rem(self.x + dx % NX, NX)


def send(src, dst, send_sem, recv_sem, target):
    pltpu.make_async_remote_copy(
        src_ref=src,
        dst_ref=dst,
        send_sem=send_sem,
        recv_sem=recv_sem,
        device_id=target,
        device_id_type=pl.DeviceIdType.MESH,
    ).start()


def arrived(ref, sem):
    pltpu.make_async_copy(ref, ref, sem).wait()


def gather(torus, buf, send_sem, recv_sem):
    def pass_on(half, dx, dz):
        source = torus.at(-dx, -dz)
        for cx, cz in children(half, dx, dz):
            send(
                buf.at[source, half],
                buf.at[source, half],
                send_sem,
                recv_sem.at[half, place(cx, cz)],
                {"kv": torus.at(cx - dx, cz - dz)},
            )

    for half in range(2):
        pass_on(half, 0, 0)
    for dx, dz in ARRIVALS:
        for half in range(2):
            arrived(buf.at[torus.at(-dx, -dz), half], recv_sem.at[half, place(dx, dz)])
            pass_on(half, dx, dz)


def sum_at_owner(torus, part, relay, column, cross, final, stage_x, stage_z, send_sem, recv_sem):
    def slot(dz):
        return dz % NZ

    for dz in DZ_FAR:
        for half in range(2):
            sign = 1 if half == 0 else -1
            send(
                part.at[torus.at(2, -dz), half],
                relay.at[half, slot(dz)],
                send_sem,
                recv_sem.at[half, slot(dz)],
                {"kv": torus.at(-sign, 0)},
            )
        for half in range(2):
            sign = 1 if half == 0 else -1
            send(
                part.at[torus.at(sign, -dz), half],
                column.at[half, 0, slot(dz)],
                send_sem,
                recv_sem.at[half, 8 + slot(dz)],
                {"kv": torus.at(sign, 0)},
            )
    for dz in DZ_FAR:
        for half in range(2):
            sign = 1 if half == 0 else -1
            arrived(relay.at[half, slot(dz)], recv_sem.at[half, slot(dz)])
            total = part[torus.at(-sign, -dz), half].astype(F32) + relay[half, slot(dz)].astype(F32)
            stage_x[half, slot(dz)] = total.astype(BF16)
            send(
                stage_x.at[half, slot(dz)],
                column.at[half, 1, slot(dz)],
                send_sem,
                recv_sem.at[half, 16 + slot(dz)],
                {"kv": torus.at(-sign, 0)},
            )
    sums = [None, None]
    for dz in DZ_FAR:
        for half in range(2):
            sign = 1 if half == 0 else -1
            arrived(column.at[half, 0, slot(dz)], recv_sem.at[half, 8 + slot(dz)])
            arrived(column.at[half, 1, slot(dz)], recv_sem.at[half, 16 + slot(dz)])
            total = (
                part[torus.at(0, -dz), half].astype(F32)
                + column[half, 0, slot(dz)].astype(F32)
                + column[half, 1, slot(dz)].astype(F32)
            )
            if dz == 0:
                sums[half] = total
                continue
            if dz == 2 * sign:
                arrived(cross.at[half], recv_sem.at[half, 28])
                total = total + cross[half].astype(F32)
            stage_z[half, slot(dz)] = total.astype(BF16)
            if dz == 4:
                send(
                    stage_z.at[half, slot(dz)],
                    cross.at[half],
                    send_sem,
                    recv_sem.at[half, 28],
                    {"kv": torus.at(0, -2 * sign)},
                )
            else:
                send(
                    stage_z.at[half, slot(dz)],
                    final.at[half, slot(dz)],
                    send_sem,
                    recv_sem.at[half, 24 + slot(dz)],
                    {"kv": torus.at(0, -dz)},
                )
    for dz in (3, -3, 2, -2, 1, -1):
        for half in range(2):
            arrived(final.at[half, slot(dz)], recv_sem.at[half, 24 + slot(dz)])
            sums[half] = sums[half] + final[half, slot(dz)].astype(F32)
    return sums


def unpack(buf, gain_ref, scaled_ref, squares_ref):
    squares_ref[...] = jnp.zeros_like(squares_ref)

    def body(k, carry):
        cols = pl.ds(pl.multiple_of(k * 128, 128), 128)
        tiles = [buf[2 * k + j // 2, j % 2].astype(F32) for j in range(4)]
        for q, tile in enumerate(lanes_swapped(tiles)):
            rows = pl.ds(64 * q, 64)
            scaled_ref[rows, cols] = (tile * gain_ref[:, cols]).astype(BF16)
            squares_ref[rows, :] += tile * tile
        return carry

    lax.fori_loop(0, D // 128, body, 0)
    total = jnp.sum(squares_ref[...], axis=1, keepdims=True)
    return lax.rsqrt(total / D + EPSILON)


def half_step(torus, buf, gain_ref, gate_ref, up_ref, down_ref, weight_waits, scaled_ref, squares_ref,
              part, sum_refs, send_sem, recv_sem):
    row_scale = unpack(buf, gain_ref, scaled_ref, squares_ref)
    for wait in weight_waits:
        wait()
    scaled = scaled_ref[...]
    gate_act = jnp.dot(scaled, gate_ref[...], preferred_element_type=F32) * row_scale
    up_act = jnp.dot(scaled, up_ref[...], preferred_element_type=F32) * row_scale
    hidden = (jax.nn.silu(gate_act) * up_act).astype(BF16)

    def body(k, carry):
        cols = pl.ds(pl.multiple_of(k * 256, 256), 256)
        product = jnp.dot(hidden, down_ref[:, cols], preferred_element_type=F32)
        for side in range(2):
            tiles = [product[64 * q : 64 * q + 64, 128 * side : 128 * side + 128] for q in range(4)]
            for j, tile in enumerate(lanes_swapped(tiles)):
                part[4 * k + 2 * side + j // 2, j % 2] = tile.astype(BF16)
        return carry

    lax.fori_loop(0, D // 256, body, 0)
    return sum_at_owner(torus, part, *sum_refs, send_sem, recv_sem)


def spread(rows, first):
    parts = [jnp.broadcast_to(rows[:, first + h : first + h + 1], (BLK, 128)) for h in range(HEADS)]
    return jnp.concatenate(parts, axis=0)


def delta(owned, gates_in, rates, live, state, fresh):
    query, key, value, gating = owned
    write_rows = jax.nn.sigmoid(gates_in) * live
    forget_rows = -jnp.exp(rates) * jax.nn.softplus(gates_in) * live
    write = spread(write_rows, 0)
    forget = spread(forget_rows, HEADS)
    query_unit = query * lax.rsqrt(jnp.sum(query * query, axis=1, keepdims=True) + EPSILON)
    query_unit = query_unit / math.sqrt(HEAD)
    key_unit = key * lax.rsqrt(jnp.sum(key * key, axis=1, keepdims=True) + EPSILON)
    row = lax.broadcasted_iota(jnp.int32, (128, 128), 0)
    col = lax.broadcasted_iota(jnp.int32, (128, 128), 1)
    same = (row >> 3) == (col >> 3)
    causal = same & (col <= row)
    strict = same & (col < row)
    identity = jnp.where(row == col, 1.0, 0.0)

    def dot(a, b):
        return jnp.dot(a, b, precision=HIGH, preferred_element_type=F32)

    def dot_nt(a, b):
        return lax.dot_general(
            a, b, (((1,), (1,)), ((), ())), precision=HIGH, preferred_element_type=F32
        )

    cumulative = dot(jnp.where(causal, 1.0, 0.0), forget)
    decay = jnp.where(causal, jnp.exp(jnp.minimum(cumulative - cumulative.T, 0.0)), 0.0)
    strict_part = jnp.where(strict, write * decay * dot_nt(key_unit, key_unit), 0.0)
    squared = dot(strict_part, strict_part)
    fourth = dot(squared, squared)
    inverse = dot(dot(identity - strict_part, identity + squared), identity + fourth)
    growth = jnp.exp(cumulative)
    target = dot(inverse, write * value)
    key_mix = dot(inverse, write * growth * key_unit)
    scores = dot_nt(query_unit, key_unit) * decay
    grown = query_unit * growth
    by_head = cumulative.reshape(HEADS, BLK, 128)
    last = by_head[:, BLK - 1 : BLK, :]
    fading = jnp.exp(last - by_head).reshape(128, 128)
    faded = key_unit * fading
    kept = jnp.exp(last)
    updates, reads = [], []
    for h in range(HEADS):
        rows = slice(8 * h, 8 * h + 8)
        both = jnp.concatenate([key_mix[rows], grown[rows]], axis=0)
        seen = dot(both, state[h])
        update = target[rows] - seen[:BLK]
        updates.append(update)
        reads.append(seen[BLK:])
        gained = lax.dot_general(
            faded[rows], update, (((0,), (0,)), ((), ())), precision=HIGH, preferred_element_type=F32
        )
        fresh[h] = kept[h] * state[h] + gained
    attend = jnp.concatenate(reads, axis=0) + dot(scores, jnp.concatenate(updates, axis=0))
    normed = attend * lax.rsqrt(jnp.mean(attend * attend, axis=1, keepdims=True) + EPSILON)
    return normed * jax.nn.silu(gating) * jnp.concatenate([live] * HEADS, axis=0)


def layer(
    tok, live, rates, gain_first, gain_mix, gain_second,
    gate1, up1, down1, gate2, up2, down2, proj, outw, wf, state,
    out, new_state,
    buf_a, buf_c, buf_m, buf_g, scaled, squares, part1, part2,
    relay1, column1, cross1, final1, relay2, column2, cross2, final2,
    stage_x1, stage_z1, stage_x2, stage_z2,
    v_gate1, v_up1, v_down1, v_gate2, v_up2, v_down2, v_proj, v_out, v_wf, v_state, v_fresh,
    outgoing, incoming, gates, last_stage,
    local_sem, send_sem, recv_ag, recv_rs, recv_x, pair_sem,
):
    torus = Torus()
    kv, tp = torus.kv, torus.tp
    other = 1 - tp

    loads = {}
    for n, (name, src, dst) in enumerate(
        [
            ("gate1", gate1, v_gate1), ("up1", up1, v_up1), ("down1", down1, v_down1),
            ("proj", proj, v_proj.at[tp]), ("out", outw, v_out.at[tp]), ("wf", wf, v_wf),
            ("state", state, v_state),
            ("gate2", gate2, v_gate2), ("up2", up2, v_up2), ("down2", down2, v_down2),
        ]
    ):
        loads[name] = pltpu.make_async_copy(src, dst, local_sem.at[n])
        loads[name].start()

    barrier = pltpu.get_barrier_semaphore()
    for d in range(1, CHIPS):
        pl.semaphore_signal(
            barrier, inc=1, device_id={"kv": lax.rem(kv + d, CHIPS)}, device_id_type=pl.DeviceIdType.MESH
        )
    pl.semaphore_signal(barrier, inc=1, device_id={"tp": other}, device_id_type=pl.DeviceIdType.MESH)
    pl.semaphore_wait(barrier, CHIPS)

    send(tok.at[other], buf_a.at[kv, tp], pair_sem.at[0], pair_sem.at[1], {"tp": other})
    buf_a[kv, tp] = tok[tp]
    arrived(buf_a.at[kv, other], pair_sem.at[1])
    gather(torus, buf_a, send_sem.at[0], recv_ag.at[0])
    loads["proj"].wait()
    loads["out"].wait()
    send(v_proj.at[tp], v_proj.at[tp], pair_sem.at[2], pair_sem.at[3], {"tp": other})
    send(v_out.at[tp], v_out.at[tp], pair_sem.at[4], pair_sem.at[5], {"tp": other})

    sums = half_step(
        torus, buf_a, gain_first, v_gate1, v_up1, v_down1,
        [loads["gate1"].wait, loads["up1"].wait, loads["down1"].wait],
        scaled, squares, part1, (relay1, column1, cross1, final1, stage_x1, stage_z1),
        send_sem.at[1], recv_rs.at[0],
    )
    for half in range(2):
        buf_c[kv, half] = (buf_a[kv, half].astype(F32) + 0.5 * sums[half]).astype(BF16)

    gather(torus, buf_c, send_sem.at[2], recv_ag.at[1])
    mix_scale = unpack(buf_c, gain_mix, scaled, squares)
    arrived(v_proj.at[other], pair_sem.at[3])
    loads["wf"].wait()
    mix_in = scaled[...]
    for t in range(2):
        product = jnp.dot(mix_in, v_proj[t], preferred_element_type=F32) * mix_scale
        outgoing[:, t] = product.reshape(CHIPS, BLK, 128).astype(BF16)
    gates[...] = jnp.dot(mix_in, v_wf[...], preferred_element_type=F32) * mix_scale
    for d in range(1, CHIPS):
        peer = lax.rem(kv + d, CHIPS)
        send(outgoing.at[peer], incoming.at[kv], send_sem.at[3], recv_x.at[d], {"kv": peer})
    incoming[kv] = outgoing[kv]
    gates_in = gates[pl.ds(pl.multiple_of(kv * BLK, BLK), BLK), :]
    loads["state"].wait()
    for d in range(1, CHIPS):
        arrived(incoming.at[lax.rem(kv + CHIPS - d, CHIPS)], recv_x.at[d])
    tiles = incoming[...].astype(F32).reshape(HEADS, 4, BLK, 128)
    owned = lanes_swapped([tiles[:, j].reshape(128, 128) for j in range(4)])
    mixed = delta(owned, gates_in, rates[...], live[...], v_state, v_fresh)
    for h in range(HEADS):
        lanes = slice(128 * (h % 8), 128 * (h % 8) + 128)
        buf_m[kv, h // 8, :, lanes] = mixed[8 * h : 8 * h + 8].astype(BF16)
    save = pltpu.make_async_copy(v_fresh, new_state, local_sem.at[10])
    save.start()

    gather(torus, buf_m, send_sem.at[4], recv_ag.at[2])
    arrived(v_out.at[other], pair_sem.at[5])
    mixes = [jnp.zeros((64, 128), F32), jnp.zeros((64, 128), F32)]
    weight = v_out[0] + v_out[1]
    for half in range(2):
        heads_half = buf_m[:, half].astype(F32).reshape(ROWS, D // 2).astype(BF16)
        product = jnp.dot(
            heads_half, weight[half * (D // 2) : (half + 1) * (D // 2)], preferred_element_type=F32
        )
        tiles = lanes_swapped([product[64 * q : 64 * q + 64] for q in range(4)])
        for t in range(2):
            mixes[t] = mixes[t] + tiles[t].astype(BF16).astype(F32)
    for half in range(2):
        buf_g[kv, half] = (buf_c[kv, half].astype(F32) + mixes[half]).astype(BF16)

    gather(torus, buf_g, send_sem.at[5], recv_ag.at[3])
    sums = half_step(
        torus, buf_g, gain_second, v_gate2, v_up2, v_down2,
        [loads["gate2"].wait, loads["up2"].wait, loads["down2"].wait],
        scaled, squares, part2, (relay2, column2, cross2, final2, stage_x2, stage_z2),
        send_sem.at[6], recv_rs.at[1],
    )
    for half in range(2):
        last_stage[half] = (buf_g[kv, half].astype(F32) + 0.5 * sums[half]).astype(BF16)
    send(last_stage.at[other], out.at[tp], pair_sem.at[6], pair_sem.at[7], {"tp": other})
    out[tp] = last_stage[tp]
    arrived(out.at[other], pair_sem.at[7])

    arrived(tok.at[other], pair_sem.at[0])
    arrived(v_proj.at[tp], pair_sem.at[2])
    arrived(v_out.at[tp], pair_sem.at[4])
    arrived(last_stage.at[other], pair_sem.at[6])
    everything = pl.ds(0, CHIPS - 1)
    for n, ref in ((0, buf_a), (1, part1), (2, buf_c), (3, incoming), (4, buf_m), (5, buf_g), (6, part2)):
        arrived(ref.at[everything], send_sem.at[n])
    save.wait()


def run_layer(*arrays):
    bf, fl = BF16, F32
    dma = pltpu.SemaphoreType.DMA
    whole = (CHIPS, 2, 64, 128)
    in_vmem = pl.BlockSpec(memory_space=pltpu.VMEM)
    in_hbm = pl.BlockSpec(memory_space=pl.ANY)
    ff = 176
    sum_set = [
        pltpu.VMEM((2, 8, 64, 128), bf), pltpu.VMEM((2, 2, 8, 64, 128), bf),
        pltpu.VMEM((2, 64, 128), bf), pltpu.VMEM((2, 8, 64, 128), bf),
    ]
    return pl.pallas_call(
        layer,
        out_shape=(
            jax.ShapeDtypeStruct((2, 64, 128), bf),
            jax.ShapeDtypeStruct((HEADS, HEAD, HEAD), fl),
        ),
        in_specs=[in_vmem] * 6 + [in_hbm] * 10,
        out_specs=(in_vmem, in_hbm),
        scratch_shapes=[
            pltpu.VMEM(whole, bf), pltpu.VMEM(whole, bf),
            pltpu.VMEM((CHIPS, 2, BLK, D // 2), bf), pltpu.VMEM(whole, bf),
            pltpu.VMEM((ROWS, D), bf), pltpu.VMEM((ROWS, 128), fl),
            pltpu.VMEM(whole, bf), pltpu.VMEM(whole, bf),
            *sum_set, *sum_set,
            *([pltpu.VMEM((2, 8, 64, 128), bf)] * 4),
            pltpu.VMEM((D, ff), bf), pltpu.VMEM((D, ff), bf), pltpu.VMEM((ff, D), bf),
            pltpu.VMEM((D, ff), bf), pltpu.VMEM((D, ff), bf), pltpu.VMEM((ff, D), bf),
            pltpu.VMEM((2, D, 128), bf), pltpu.VMEM((2, D, 128), bf), pltpu.VMEM((D, 128), bf),
            pltpu.VMEM((HEADS, HEAD, HEAD), fl), pltpu.VMEM((HEADS, HEAD, HEAD), fl),
            pltpu.VMEM((CHIPS, 2, BLK, 128), bf), pltpu.VMEM((CHIPS, 2, BLK, 128), bf),
            pltpu.VMEM((ROWS, 128), fl), pltpu.VMEM((2, 64, 128), bf),
            dma((11,)), dma((7,)), dma((4, 2, 32)), dma((2, 2, 32)), dma((32,)), dma((8,)),
        ],
        compiler_params=pltpu.CompilerParams(
            collective_id=0, has_side_effects=True, vmem_limit_bytes=56 * 1024 * 1024
        ),
        name="layer",
    )(*arrays)


def per_device(
    tokens,
    lengths,
    state,
    gain_first,
    first_gate,
    first_up,
    first_down,
    gain_mix,
    query_weight,
    key_weight,
    value_weight,
    gating_weight,
    write_weight,
    forget_weight,
    forget_rate,
    out_weight,
    gain_second,
    second_gate,
    second_up,
    second_down,
):
    tok = tokens.reshape(4, 8, 2, BLK, 32).transpose(2, 1, 3, 0, 4).reshape(2, 64, 128)
    live = (jnp.arange(BLK, dtype=jnp.int32) < lengths[0]).astype(F32)
    live = jnp.broadcast_to(live[:, None], (BLK, 128))
    rates = jnp.pad(forget_rate[None, :], ((0, 0), (HEADS, 128 - 2 * HEADS)))
    proj = jnp.concatenate([query_weight, key_weight, value_weight, gating_weight], axis=1)
    blank = jnp.zeros_like(out_weight)
    first = lax.axis_index("tp") == 0
    outw = jnp.concatenate(
        [jnp.where(first, out_weight, blank), jnp.where(first, blank, out_weight), blank, blank], axis=1
    )
    wf = jnp.pad(
        jnp.concatenate([write_weight, forget_weight], axis=1), ((0, 0), (0, 128 - 2 * HEADS))
    )
    out, new_state = run_layer(
        tok, live, rates, gain_first[None, :], gain_mix[None, :], gain_second[None, :],
        first_gate, first_up, first_down, second_gate, second_up, second_down,
        proj, outw, wf, state.reshape(HEADS, HEAD, HEAD),
    )
    mixed_out = out.reshape(2, 8, BLK, 4, 32).transpose(3, 1, 0, 2, 4).reshape(512, 32)
    return mixed_out, new_state.reshape(state.shape)


def solution(mesh):
    in_specs = (
        P("dp", ("kv", "tp")),
        P(("dp", "kv", "tp")),
        P(("dp", "kv", "tp"), None, None, None),
        P(),
        P(None, "kv"),
        P(None, "kv"),
        P("kv", None),
        P(),
        P(None, ("kv", "tp")),
        P(None, ("kv", "tp")),
        P(None, ("kv", "tp")),
        P(None, ("kv", "tp")),
        P(),
        P(),
        P(),
        P(None, ("kv", "tp")),
        P(),
        P(None, "kv"),
        P(None, "kv"),
        P("kv", None),
    )
    out_specs = (P("dp", ("kv", "tp")), P(("dp", "kv", "tp"), None, None, None))
    return jax.shard_map(
        per_device, mesh=mesh, in_specs=in_specs, out_specs=out_specs, check_vma=False
    )
```

time: 315 us -> 168 us (0.53)
  blocking collectives: 178 us -> 0 us
  Pallas kernels: 0 us -> 147 us
  waiting for transfers between devices: 79.8 us -> 0 us
  starting transfers between devices: 19.1 us -> 0 us
  matrix products: 19 us -> 0 us
  local copies, waits for them, and re-layouts: 11.6 us -> 17.2 us
  other arithmetic: 5.37 us -> 2.05 us
    all_to_all x8 -> x0, blocking collectives: 178 us -> none  [the longest x3 120 us: copy_for_each(): return lax.all_to_all(copies, axis, split_axis=0, concat_axis=0, tiled=True)]
    pallas_call x0 -> x1, Pallas kernels: none -> 147 us  [run_layer(): pl.pallas_call(layer, out_shape=(jax.ShapeDtypeStruct((2, 64, 128), bf),...]
    all_to_all x3 -> x0, waiting for transfers between devices: 79.8 us -> none  [the longest x1 49 us: copy_for_each(): return lax.all_to_all(copies, axis, split_axis=0, concat_axis=0, tiled=True)]
    all_to_all x3 -> x0, starting transfers between devices: 19.1 us -> none  [the longest x1 6.97 us: per_device(): lax.all_to_all(stacked.astype(jnp.bfloat16), ('kv', 'tp'), split_axis=1,...]
    dot_general x24 -> x0, matrix products: 19 us -> none  [the longest x2 5.75 us: finish_units(): return jnp.dot(hidden, down_rows, preferred_element_type=jnp.float32)]
    unnamed x32 -> x36, local copies, waits for them, and re-layouts: 3.71 us -> 12.3 us
    convert_element_type x9 -> x1, other arithmetic: 3.55 us -> 0.01 us  [per_device(): live = (jnp.arange(BLK, dtype=jnp.int32) < lengths[0]).astype(F32)]
  transfers between devices with their start and end apart: 3 -> 0, of which waited for: 3 -> 0; matrix products, arithmetic and copies ran while one was open for 2% -> 0% of each run, Pallas kernels for 0% -> 0%
where the time goes in v1:
time: 168 us
  Pallas kernels  147 us (88%)
  local copies, waits for them, and re-layouts  17.2 us (10%)
  other arithmetic  2.05 us (1%)
    pallas_call x1, Pallas kernels, run_layer(): pl.pallas_call(layer, out_shape=(jax.ShapeDtypeStruct((2, 64, 128), bf),...  147 us
    unnamed x36, local copies, waits for them, and re-layouts  12.3 us

profile of v1, /device:TPU:1, one launch (start us, length us, event | category | flops | bytes accessed | tf_op | source)
XLA Modules:
  0.0 167.9 jit_solution(11915517273500476994)
XLA Ops:
  0.6 0.0 copy-start.11
  1.3 1.2 pad.8.rates
  2.5 0.1 pad.14.clone
  2.6 0.7 broadcast_in_dim.21.live
  3.3 0.0 copy-done.11
  3.3 0.1 copy.52
  3.4 0.1 copy.53
  3.5 0.0 copy-start.9
  3.5 0.0 copy-start.10
  3.5 0.7 reshape.28.tok
  4.3 0.1 copy-done.9
  4.4 0.0 copy-done.10
  4.4 0.3 copy.60
  4.7 0.0 copy-start.4
  4.7 0.9 pad.9.wf
  5.6 0.0 copy-done.4
  5.6 0.0 copy-start.5
  5.7 0.3 copy.54
  5.9 0.6 copy-done.5
  6.6 0.0 copy-start.6
  6.6 0.3 copy.55
  6.8 0.6 copy-done.6
  7.5 0.0 copy-start.7
  7.5 0.3 copy.56
  7.7 0.6 copy-done.7
  8.4 0.0 copy-start.8
  8.4 0.3 copy.57
  8.6 0.6 copy-done.8
  9.3 0.3 copy.58
  9.5 0.1 broadcast_select_fusion.1
  9.6 0.0 copy-start
  9.6 2.0 %pad_maximum_fusion = (bf16[2048,128]{1,0:T(8,128)(2,1)}, bf16[2048,128]{1,0:T(8,128)(2,1)}) fusion(bf16[2048,32]{1,0:T(8,128)(2,1)S(1)} %copy.57, bf16[2048,32]{1,0:T(8,128)(2,1)S(1)} %copy.56, bf16[2048,32]{1,0:T(8,128)(2,1)S(1)} %copy.55, bf16[2048,32]{1,0:T(8,128)(2,1)S(1)} %copy.54, bf16[128]{0:T(256)(128)(2,1)S(1)} %pad.14.clone, ...), kind=kLoop, calls=%fused_computation | loop fusion | flops 3670016 | bytes 1835264 | tf_op jit(solution)/shard_map/concatenate | solution.py:482
  11.6 0.0 copy-done
  11.6 0.0 copy-start.1
  11.6 1.3 copy.61.gate1
  12.9 0.0 copy-done.1
  12.9 0.0 copy-start.2
  12.9 1.3 copy.62.up1
  14.2 0.0 copy-done.2
  14.2 0.0 copy-start.3
  14.2 1.3 copy.63.gate2
  15.5 0.0 copy-done.3
  15.5 1.3 copy.64.up2
  16.8 147.2 %layer.1 = (bf16[2,64,128]{2,1,0:T(8,128)(2,1)}, f32[16,128,128]{2,1,0:T(8,128)}) custom-call(bf16[2,64,128]{2,1,0:T(8,128)(2,1)} %reshape.28.tok, f32[8,128]{1,0:T(8,128)} %broadcast_in_dim.21.live, f32[1,128]{1,0:T(1,128)} %pad.8.rates, f32[1,2048]{1,0:T(1,128)} %bitcast.18, f32[1,2048]{1,0:T(1,128)} %bitcast.19, f32[1,2048]{1,0:T(1,128)} %bitcast.20, ...), custom_call_target="tpu_custom_call" | custom-call | tf_op jit(solution)/shard_map/layer/pallas_call | solution.py:426
  164.0 0.9 reshape.30
  164.9 0.7 copy.66
  165.6 2.3 %copy.69 = f32[1,16,128,128]{3,2,1,0:T(8,128)} copy(f32[1,16,128,128]{3,2,1,0:T(8,128)} %bitcast.15) | data formatting | bytes 2097152
  (4 shorter events, 0.0 us)
Async XLA Ops:
  0.6 2.7 %copy-start.11 = (bf16[512,32]{0,1:T(8,128)(2,1)S(1)}, bf16[512,32]{0,1:T(8,128)(2,1)}, u32[]{:S(2)}) copy-start(bf16[512,32]{0,1:T(8,128)(2,1)} %param.20) | copy-start | bytes 98308
  3.5 0.8 copy-start.9
  3.5 0.9 copy-start.10
  4.7 1.0 copy-start.4
  5.6 0.9 copy-start.5
  6.6 0.9 copy-start.6
  7.5 0.9 copy-start.7
  8.4 0.9 copy-start.8
  9.6 2.0 %copy-start = (bf16[2048,176]{0,1:T(8,128)(2,1)S(1)}, bf16[2048,176]{0,1:T(8,128)(2,1)}, u32[]{:S(2)}) copy-start(bf16[2048,176]{0,1:T(8,128)(2,1)} %param.24) | copy-start | bytes 2162692
  11.6 1.3 copy-start.1
  12.9 1.3 copy-start.2
  14.2 1.3 copy-start.3

commit v2 on v1

v2 whole, which is shorter than its diff:
```python
import math

import jax
import jax.numpy as jnp
from jax import lax
from jax.experimental import pallas as pl
from jax.experimental.pallas import tpu as pltpu
from jax.sharding import PartitionSpec as P

HEADS = 16
HEAD = 128
BLK = 8
D = 2048
NX = 4
NZ = 8
CHIPS = NX * NZ
ROWS = CHIPS * BLK
EPSILON = 1e-06
F32 = jnp.float32
BF16 = jnp.bfloat16
HIGH = lax.Precision.HIGHEST


def lanes_swapped(tiles):
    rows = tiles[0].shape[0]
    lane = lax.broadcasted_iota(jnp.int32, (rows, 128), 1)
    out = list(tiles)
    for step in (2, 1):
        width = step * 32
        low = (lane & width) == 0
        for i in range(4):
            if i & step:
                continue
            a, b = out[i], out[i + step]
            out[i] = jnp.where(low, a, pltpu.roll(b, width, 1))
            out[i + step] = jnp.where(low, pltpu.roll(a, 128 - width, 1), b)
    return out


def dot_nt(a, b, precision=None):
    return lax.dot_general(
        a, b, (((1,), (1,)), ((), ())), precision=precision, preferred_element_type=F32
    )


def wrapped(dz):
    return (dz + 3) % NZ - 3


def place(dx, dz):
    return (dx % NX) * NZ + dz % NZ


def children(half, dx, dz):
    dx, dz = dx % NX, wrapped(dz)
    if abs(dz) == 1:
        return []
    found = []
    if dx == 0:
        if dz == 0:
            found += [(0, 4)]
        if half == 0:
            found += [(2, dz)]
        found += [(-1, dz), (1, dz)]
        if dz == 0:
            found += [(0, 2), (0, -2), (0, 3), (0, -3), (0, 1), (0, -1)]
    else:
        if half == 1 and dx == NX - 1:
            found += [(2, dz)]
        if dz == 0:
            found += [(dx, 1), (dx, -1)]
    return found


GATHER_STEPS = (
    ("side", 0), ("column", 2), ("column", -2), ("far", 0), ("column", 3), ("column", -3), ("column", 4),
    ("relay", 2), ("row", 0), ("relay", -2), ("relay", 3), ("row", 1), ("relay", -3), ("relay", 4),
    ("row", -1), ("row", 2), ("row", -2), ("row", 3), ("row", -3), ("row", 4),
)
SUM_STEPS = (
    ("produce", 4), ("produce", 1), ("produce", -1), ("produce", 3), ("produce", -3),
    ("produce", 2), ("produce", -2), ("produce", 0),
    ("relay", 4), ("relay", 3), ("relay", -3), ("cross_row", 0), ("relay", 2), ("column", 4),
    ("relay", -2), ("column", 3), ("column", -3), ("relay", 0), ("column", 2), ("column", -2), ("column", 0),
)


class Torus:
    def __init__(self):
        self.kv = lax.axis_index("kv")
        self.tp = lax.axis_index("tp")
        self.x = lax.rem(self.kv, NX)
        self.z = lax.div(self.kv, NX)

    def at(self, dx, dz):
        return lax.rem(self.z + dz % NZ, NZ) * NX + lax.rem(self.x + dx % NX, NX)


def send(src, dst, send_sem, recv_sem, target):
    pltpu.make_async_remote_copy(
        src_ref=src,
        dst_ref=dst,
        send_sem=send_sem,
        recv_sem=recv_sem,
        device_id=target,
        device_id_type=pl.DeviceIdType.MESH,
    ).start()


def arrived(ref, sem):
    pltpu.make_async_copy(ref, ref, sem).wait()


def gather(torus, buf, send_sem, recv_sem, consume=None):
    def pass_on(half, dx, dz):
        source = torus.at(-dx, -dz)
        for cx, cz in children(half, dx, dz):
            send(
                buf.at[source, half],
                buf.at[source, half],
                send_sem,
                recv_sem.at[half, place(cx, cz)],
                {"kv": torus.at(cx - dx, cz - dz)},
            )

    def take(half, dx, dz):
        arrived(buf.at[torus.at(-dx, -dz), half], recv_sem.at[half, place(dx, dz)])
        pass_on(half, dx, dz)

    for half in range(2):
        pass_on(half, 0, 0)
    for what, dz in GATHER_STEPS:
        if what == "column":
            take(0, 0, dz)
            take(1, 0, dz)
        elif what == "side":
            for dx in (1, -1):
                take(0, dx, 0)
                take(1, dx, 0)
        elif what == "far":
            take(0, 2, 0)
            take(1, 2, 0)
        elif what == "relay":
            take(1, -1, dz)
        else:
            if abs(dz) == 1:
                places = [(half, dx) for dx in (0, 1, -1, 2) for half in range(2)]
            elif dz != 0:
                places = [(0, -1), (0, 1), (1, 1), (0, 2), (1, 2)]
            else:
                places = []
            for half, dx in places:
                take(half, dx, dz)
            if consume is not None:
                consume(lax.rem(torus.z + (-dz) % NZ, NZ))


def sum_at_owner(
    torus, part, relay, column, final, along_z, stage_x, stage_z, stage_row, send_sem, recv_sem, produce
):
    sums = [None, None]

    def slot(dz):
        return dz % NZ

    def z_slot(dx, dz):
        return (dx % NX) + (0 if dz == 1 else NX)

    def term(half, dx, dz):
        total = part[torus.at(-dx, -dz), half].astype(F32)
        if dz == 0 and dx != 0:
            for side in (1, -1):
                total = total + along_z[half, z_slot(dx, side)].astype(F32)
        return total

    def post(src, dst, half, place_at, target):
        send(src, dst, send_sem, recv_sem.at[half, place_at], {"kv": target})

    def produce_step(dz):
        produce(lax.rem(torus.z + (-dz) % NZ, NZ))
        for half in range(2):
            if abs(dz) == 1:
                for dx in (2, 1, -1):
                    n = z_slot(dx, dz)
                    post(part.at[torus.at(-dx, -dz), half], along_z.at[half, n], half, 32 + n, torus.at(0, -dz))
                post(
                    part.at[torus.at(0, -dz), half], final.at[half, slot(dz)], half, 24 + slot(dz), torus.at(0, -dz)
                )
            elif dz != 0:
                for dx in (2, 1, -1):
                    to_column(half, dx, dz, part.at[torus.at(-dx, -dz), half])

    def to_column(half, dx, dz, src):
        if half == 1 and dx == 2:
            post(src, relay.at[slot(dz)], half, slot(dz), torus.at(1, 0))
        elif half == 0 or dx == 1:
            n = {2: 2, 1: 0, -1: 1}[dx]
            post(src, column.at[half, n, slot(dz)], half, (8, 16, 0)[n] + slot(dz), torus.at(-dx, 0))

    def cross_row_step():
        for half in range(2):
            for dx in (2, 1, -1):
                for side in (1, -1):
                    n = z_slot(dx, side)
                    arrived(along_z.at[half, n], recv_sem.at[half, 32 + n])
        for half, dx in ((1, 2), (0, 2), (0, 1), (0, -1), (1, 1)):
            stage_row[half, dx % NX] = term(half, dx, 0).astype(BF16)
            to_column(half, dx, 0, stage_row.at[half, dx % NX])

    def relay_step(dz):
        arrived(relay.at[slot(dz)], recv_sem.at[1, slot(dz)])
        total = term(1, -1, dz) + relay[slot(dz)].astype(F32)
        stage_x[slot(dz)] = total.astype(BF16)
        post(stage_x.at[slot(dz)], column.at[1, 1, slot(dz)], 1, 16 + slot(dz), torus.at(1, 0))

    def column_step(half, dz):
        total = term(half, 0, dz)
        for n in range(3 - half):
            arrived(column.at[half, n, slot(dz)], recv_sem.at[half, (8, 16, 0)[n] + slot(dz)])
            total = total + column[half, n, slot(dz)].astype(F32)
        if dz == 0:
            sums[half] = total
            return
        stage_z[half, slot(dz)] = total.astype(BF16)
        post(stage_z.at[half, slot(dz)], final.at[half, slot(dz)], half, 24 + slot(dz), torus.at(0, -dz))

    for what, dz in SUM_STEPS:
        if what == "produce":
            produce_step(dz)
        elif what == "cross_row":
            cross_row_step()
        elif what == "relay":
            relay_step(dz)
        else:
            column_step(0, dz)
            column_step(1, dz)
    for dz in (1, -1, 4, 3, -3, 2, -2):
        for half in range(2):
            arrived(final.at[half, slot(dz)], recv_sem.at[half, 24 + slot(dz)])
            sums[half] = sums[half] + final[half, slot(dz)].astype(F32)
    return sums


def renew(h, state, fresh, update_refs):
    rows = slice(8 * h, 8 * h + 8)
    faded_ref, update_ref, kept_ref = update_refs
    gained = lax.dot_general(
        faded_ref[rows], update_ref[rows], (((0,), (0,)), ((), ())), precision=HIGH, preferred_element_type=F32
    )
    fresh[h] = kept_ref[8 * h : 8 * h + 1, :] * state[h] + gained


def unpack_row(buf, gain_ref, scaled_ref, squares_ref, zt):
    for tile in range(2):
        gain = gain_ref[:, pl.ds(pl.multiple_of(zt * 256 + 128 * tile, 128), 128)]
        for odd in range(2):
            for half in range(2):
                rows = slice(128 * odd + 64 * half, 128 * odd + 64 * half + 64)
                value = buf[4 * zt + 2 * tile + odd, half].astype(F32)
                scaled_ref[rows, 128 * tile : 128 * tile + 128] = (value * gain).astype(BF16)
                squares_ref[rows, :] += value * value


def scale_of(squares_ref):
    return lax.rsqrt(jnp.sum(squares_ref[...], axis=1, keepdims=True) / D + EPSILON)


def half_step(torus, buf, gain_ref, gate_ref, up_ref, down_ref, weight_waits, scaled_ref, squares_ref,
              acts, part, sum_refs, gather_sems, sum_sems, gathered=None):
    gate_act, up_act = acts
    squares_ref[...] = jnp.zeros_like(squares_ref)
    gate_act[...] = jnp.zeros_like(gate_act)
    up_act[...] = jnp.zeros_like(up_act)
    for wait in weight_waits:
        wait()

    def consume(zt):
        unpack_row(buf, gain_ref, scaled_ref, squares_ref, zt)
        channels = pl.ds(pl.multiple_of(zt * 256, 256), 256)
        scaled = scaled_ref[...]
        gate_act[...] += dot_nt(scaled, gate_ref[:, channels])
        up_act[...] += dot_nt(scaled, up_ref[:, channels])

    with jax.named_scope("gather"):
        gather(torus, buf, *gather_sems, consume)
    if gathered is not None:
        gathered()
    with jax.named_scope("units"):
        row_scale = scale_of(squares_ref)
        hidden = (jax.nn.silu(gate_act[...] * row_scale) * (up_act[...] * row_scale)).astype(BF16)

    def produce(zt):
        cols = pl.ds(pl.multiple_of(zt * 256, 256), 256)
        product = jnp.dot(hidden, down_ref[:, cols], preferred_element_type=F32)
        for tile in range(2):
            for odd in range(2):
                for half in range(2):
                    row = 128 * odd + 64 * half
                    block = product[row : row + 64, 128 * tile : 128 * tile + 128]
                    part[4 * zt + 2 * tile + odd, half] = block.astype(BF16)

    with jax.named_scope("sum"):
        return sum_at_owner(torus, part, *sum_refs, *sum_sems, produce)


def spread(rows):
    parts = [jnp.broadcast_to(rows[:, h : h + 1], (BLK, 128)) for h in range(HEADS)]
    return jnp.concatenate(parts, axis=0)


def delta(owned, write_pre, forget_pre, rates, live, state, update_refs):
    query, key, value, gating = owned
    live_heads = live[:, :HEADS]
    write = spread(jax.nn.sigmoid(write_pre) * live_heads)
    forget = spread(-jnp.exp(rates) * jax.nn.softplus(forget_pre) * live_heads)
    query_unit = query * lax.rsqrt(jnp.sum(query * query, axis=1, keepdims=True) + EPSILON)
    query_unit = query_unit / math.sqrt(HEAD)
    key_unit = key * lax.rsqrt(jnp.sum(key * key, axis=1, keepdims=True) + EPSILON)
    row = lax.broadcasted_iota(jnp.int32, (128, 128), 0)
    col = lax.broadcasted_iota(jnp.int32, (128, 128), 1)
    same = (row >> 3) == (col >> 3)
    causal = same & (col <= row)
    strict = same & (col < row)
    identity = jnp.where(row == col, 1.0, 0.0)

    def dot(a, b):
        return jnp.dot(a, b, precision=HIGH, preferred_element_type=F32)

    cumulative = dot(jnp.where(causal, 1.0, 0.0), forget)
    decay = jnp.where(causal, jnp.exp(jnp.minimum(cumulative - cumulative.T, 0.0)), 0.0)
    strict_part = jnp.where(strict, write * decay * dot_nt(key_unit, key_unit, HIGH), 0.0)
    squared = dot(strict_part, strict_part)
    fourth = dot(squared, squared)
    inverse = dot(dot(identity - strict_part, identity + squared), identity + fourth)
    growth = jnp.exp(cumulative)
    target = dot(inverse, write * value)
    key_mix = dot(inverse, write * growth * key_unit)
    scores = dot_nt(query_unit, key_unit, HIGH) * decay
    grown = query_unit * growth
    by_head = cumulative.reshape(HEADS, BLK, 128)
    last = by_head[:, BLK - 1 : BLK, :]
    fading = jnp.exp(last - by_head).reshape(128, 128)
    faded = key_unit * fading
    kept = jnp.exp(last)
    updates, reads = [], []
    for h in range(HEADS):
        rows = slice(8 * h, 8 * h + 8)
        both = jnp.concatenate([key_mix[rows], grown[rows]], axis=0)
        seen = dot(both, state[h])
        updates.append(target[rows] - seen[:BLK])
        reads.append(seen[BLK:])
    update = jnp.concatenate(updates, axis=0)
    faded_ref, update_ref, kept_ref = update_refs
    faded_ref[...] = faded
    update_ref[...] = update
    kept_ref[...] = jnp.broadcast_to(kept, (HEADS, BLK, 128)).reshape(128, 128)
    attend = jnp.concatenate(reads, axis=0) + dot(scores, update)
    normed = attend * lax.rsqrt(jnp.mean(attend * attend, axis=1, keepdims=True) + EPSILON)
    return normed * jax.nn.silu(gating) * jnp.concatenate([live] * HEADS, axis=0)


def layer(
    length, tokens, rates, gain_first, gain_mix, gain_second,
    gate1, up1, down1, gate2, up2, down2, query, key, value, gating, outw, writew, forgetw, state,
    out, new_state,
    buf_a, buf_c, buf_m, buf_g, scaled, squares, gate_act, up_act, project, part1, part2,
    relay1, column1, final1, along1, stage_x1, stage_z1, stage_row1,
    relay2, column2, final2, along2, stage_x2, stage_z2, stage_row2,
    v_gate1, v_up1, v_down1, v_gate2, v_up2, v_down2, v_all, v_out, v_state, v_fresh, faded_s, update_s, kept_s,
    s_length, outgoing, incoming, gates, tok, tok_in, last_stage, last_in,
    local_sem, send_sem, recv_ag, recv_rs, recv_x, pair_sem, quad_send, quad_recv,
):
    torus = Torus()
    update_refs = (faded_s, update_s, kept_s)

    def own_columns(t):
        return pl.multiple_of(128 * t, 128)

    kv, tp = torus.kv, torus.tp
    other = 1 - tp
    odd = lax.rem(kv, 2)
    twin = kv + 1 - 2 * odd
    seat = 2 * odd + tp
    own_out = pl.ds(pl.multiple_of(32 * seat, 32), 32)
    quad = [
        ({"tp": other}, 2 * odd + other),
        ({"kv": twin}, 2 * (1 - odd) + tp),
        ({"kv": twin, "tp": other}, 2 * (1 - odd) + other),
    ]

    with jax.named_scope("entry"):
        barrier = pltpu.get_barrier_semaphore()
        near = [{"kv": torus.at(dx, 0)} for dx in (1, -1, 2)]
        near += [{"kv": torus.at(0, dz)} for dz in (1, -1, 2, -2, 3, -3, 4)]
        near += [{"tp": other}, {"kv": twin, "tp": other}]
        for target in near:
            pl.semaphore_signal(barrier, inc=1, device_id=target, device_id_type=pl.DeviceIdType.MESH)
        loads = {}
        for n, (name, src, dst) in enumerate(
            [
                ("gate1", gate1, v_gate1), ("up1", up1, v_up1), ("down1", down1, v_down1),
                ("query", query, v_all.at[pl.ds(own_columns(tp), 32)]),
                ("key", key, v_all.at[pl.ds(own_columns(tp) + 32, 32)]),
                ("value", value, v_all.at[pl.ds(own_columns(tp) + 64, 32)]),
                ("gating", gating, v_all.at[pl.ds(own_columns(tp) + 96, 32)]),
                ("out", outw, v_out.at[own_out]),
                ("write", writew, v_all.at[256:272]), ("forget", forgetw, v_all.at[272:288]),
                ("state", state, v_state),
                ("length", length, s_length), ("gate2", gate2, v_gate2), ("up2", up2, v_up2), ("down2", down2, v_down2),
            ]
        ):
            loads[name] = pltpu.make_async_copy(src, dst, local_sem.at[n])
            loads[name].start()

        values = tokens[...].astype(F32)
        values = jnp.concatenate([values[:, 128 * q : 128 * q + 128] for q in range(4)], axis=0).T
        values = values.reshape(8, 2, BLK, 128)
        for parity in range(2):
            tok[parity] = values[:, parity].reshape(64, 128).astype(BF16)
        pl.semaphore_wait(barrier, len(near))
    with jax.named_scope("quad_in"):
        for n, (target, _) in enumerate(quad):
            row = tp if n == 1 else other
            send(tok.at[row], tok_in.at[seat], quad_send.at[n], quad_recv.at[seat], target)
        tok_in[seat] = tok[tp]
        for _, place_at in quad:
            arrived(tok_in.at[place_at], quad_recv.at[place_at])
        tiles = lanes_swapped([tok_in[j].astype(F32) for j in range(4)])
        for half in range(2):
            buf_a[kv, half] = jnp.where(odd == 0, tiles[half], tiles[2 + half]).astype(BF16)
    mine = v_all.at[pl.ds(own_columns(tp), 128)]

    def share_projections():
        for name in ("query", "key", "value", "gating"):
            loads[name].wait()
        loads["out"].wait()
        for n, (target, _) in enumerate(quad[:2]):
            send(v_out.at[own_out], v_out.at[own_out], quad_send.at[3 + n], quad_recv.at[4 + seat], target)
        send(mine, mine, pair_sem.at[0], pair_sem.at[1], {"tp": other})

    sums = half_step(
        torus, buf_a, gain_first, v_gate1, v_up1, v_down1,
        [loads["gate1"].wait, loads["up1"].wait, loads["down1"].wait],
        scaled, squares, (gate_act, up_act), part1,
        (relay1, column1, final1, along1, stage_x1, stage_z1, stage_row1),
        (send_sem.at[0], recv_ag.at[0]), (send_sem.at[1], recv_rs.at[0]), share_projections,
    )
    for half in range(2):
        buf_c[kv, half] = (buf_a[kv, half].astype(F32) + 0.5 * sums[half]).astype(BF16)

    arrived(v_all.at[pl.ds(own_columns(other), 128)], pair_sem.at[1])
    loads["write"].wait()
    loads["forget"].wait()
    squares[...] = jnp.zeros_like(squares)
    project[...] = jnp.zeros_like(project)

    def consume(zt):
        unpack_row(buf_c, gain_mix, scaled, squares, zt)
        channels = pl.ds(pl.multiple_of(zt * 256, 256), 256)
        project[...] += dot_nt(scaled[...], v_all[:, channels])

    with jax.named_scope("gather_c"):
        gather(torus, buf_c, send_sem.at[2], recv_ag.at[1], consume)
    with jax.named_scope("project"):
        mix_scale = scale_of(squares)
        for t in range(2):
            product = project[:, 128 * t : 128 * t + 128] * mix_scale
            outgoing[:, t] = product.reshape(CHIPS, BLK, 128).astype(BF16)
        gates[...] = project[:, 256:] * mix_scale
    with jax.named_scope("exchange"):
        for d in range(1, CHIPS):
            peer = lax.rem(kv + d, CHIPS)
            send(outgoing.at[peer], incoming.at[kv], send_sem.at[3], recv_x.at[d], {"kv": peer})
        incoming[kv] = outgoing[kv]
        own_rows = pl.ds(pl.multiple_of(kv * BLK, BLK), BLK)
        loads["length"].wait()
        position = lax.broadcasted_iota(jnp.int32, (BLK, 128), 0)
        live = jnp.where(position < s_length[0], 1.0, 0.0)
        loads["state"].wait()
        for d in range(1, CHIPS):
            arrived(incoming.at[lax.rem(kv + CHIPS - d, CHIPS)], recv_x.at[d])
    twin_seat = quad[1][1]
    twin_out = v_out.at[pl.ds(pl.multiple_of(32 * twin_seat, 32), 32)]
    with jax.named_scope("delta"):
        tiles = incoming[...].astype(F32).reshape(HEADS, 4, BLK, 128)
        owned = lanes_swapped([tiles[:, j].reshape(128, 128) for j in range(4)])
        gates_in = gates[own_rows, :]
        mixed = delta(owned, gates_in[:, :HEADS], gates_in[:, HEADS:], rates[...], live, v_state, update_refs)
        for h in range(HEADS):
            lanes = slice(128 * (h % 8), 128 * (h % 8) + 128)
            buf_m[kv, h // 8, :, lanes] = mixed[8 * h : 8 * h + 8].astype(BF16)
    heads_left = list(range(HEADS))

    def renew_two(zt):
        if len(heads_left) == HEADS:
            arrived(twin_out, quad_recv.at[4 + twin_seat])
            send(twin_out, twin_out, quad_send.at[5], quad_recv.at[4 + twin_seat], {"tp": other})
        for _ in range(2):
            renew(heads_left.pop(0), v_state, v_fresh, update_refs)

    with jax.named_scope("gather_m"):
        gather(torus, buf_m, send_sem.at[4], recv_ag.at[2], renew_two)
    save = pltpu.make_async_copy(v_fresh, new_state, local_sem.at[15])
    save.start()
    with jax.named_scope("out_product"):
        for place_at in (quad[0][1], quad[2][1]):
            rows = pl.ds(pl.multiple_of(32 * place_at, 32), 32)
            arrived(v_out.at[rows], quad_recv.at[4 + place_at])
        mixed_sum = jnp.zeros((128, 128), F32)
        for half in range(2):
            lanes = slice(half * (D // 2), (half + 1) * (D // 2))
            heads_half = buf_m[pl.ds(16 * odd, 16), half].astype(F32).reshape(128, D // 2).astype(BF16)
            mixed_sum = mixed_sum + dot_nt(heads_half, v_out[:, lanes]).astype(BF16).astype(F32)
        for half in range(2):
            rows = slice(64 * half, 64 * half + 64)
            buf_g[kv, half] = (buf_c[kv, half].astype(F32) + mixed_sum[rows]).astype(BF16)

    sums = half_step(
        torus, buf_g, gain_second, v_gate2, v_up2, v_down2,
        [loads["gate2"].wait, loads["up2"].wait, loads["down2"].wait],
        scaled, squares, (gate_act, up_act), part2,
        (relay2, column2, final2, along2, stage_x2, stage_z2, stage_row2),
        (send_sem.at[5], recv_ag.at[3]), (send_sem.at[6], recv_rs.at[1]),
    )
    with jax.named_scope("finish"):
        for half in range(2):
            last_stage[half] = (buf_g[kv, half].astype(F32) + 0.5 * sums[half]).astype(BF16)
        for n, (target, _) in enumerate(quad):
            send(last_stage, last_in.at[tp, odd], quad_send.at[6 + n], quad_recv.at[8 + 2 * odd + tp], target)
        last_in[tp, odd] = last_stage[...]
        for _, place_at in quad:
            from_odd, from_tp = lax.div(place_at, 2), lax.rem(place_at, 2)
            arrived(last_in.at[from_tp, from_odd], quad_recv.at[8 + place_at])
        sides = []
        for parity in range(2):
            tiles = [last_in[parity, q // 2, q % 2].astype(F32) for q in range(4)]
            tiles = lanes_swapped(tiles)
            low = jnp.where(tp == 0, tiles[0], tiles[1])
            high = jnp.where(tp == 0, tiles[2], tiles[3])
            sides.append(jnp.where(odd == 0, low, high).reshape(8, 1, BLK, 128))
        both = jnp.concatenate(sides, axis=1).reshape(128, 128).T.astype(BF16)
        for q in range(4):
            out[:, 128 * q : 128 * q + 128] = both[32 * q : 32 * q + 32]

        arrived(mine, pair_sem.at[0])
        for n, (target, _) in enumerate(quad):
            arrived(tok.at[tp if n == 1 else other], quad_send.at[n])
            arrived(v_out.at[own_out], quad_send.at[3 + n])
            arrived(last_stage, quad_send.at[6 + n])
        everything = pl.ds(0, CHIPS - 1)
        for n, ref in (
            (0, buf_a), (1, part1), (2, buf_c), (3, incoming), (4, buf_m), (5, buf_g), (6, part2)
        ):
            arrived(ref.at[everything], send_sem.at[n])
        save.wait()


def run_layer(*arrays):
    bf, fl = BF16, F32
    dma = pltpu.SemaphoreType.DMA
    whole = (CHIPS, 2, 64, 128)
    in_vmem = pl.BlockSpec(memory_space=pltpu.VMEM)
    in_hbm = pl.BlockSpec(memory_space=pl.ANY)
    ff = 176
    eight = (8, 64, 128)
    sum_set = [
        pltpu.VMEM(eight, bf), pltpu.VMEM((2, 3, *eight), bf), pltpu.VMEM((2, *eight), bf), pltpu.VMEM((2, *eight), bf),
        pltpu.VMEM(eight, bf), pltpu.VMEM((2, *eight), bf), pltpu.VMEM((2, 4, 64, 128), bf),
    ]
    return pl.pallas_call(
        layer,
        out_shape=(
            jax.ShapeDtypeStruct((32, 512), bf),
            jax.ShapeDtypeStruct((HEADS, HEAD, HEAD), fl),
        ),
        in_specs=[in_hbm] + [in_vmem] * 5 + [in_hbm] * 14,
        out_specs=(in_vmem, in_hbm),
        scratch_shapes=[
            pltpu.VMEM(whole, bf), pltpu.VMEM(whole, bf),
            pltpu.VMEM((CHIPS, 2, BLK, D // 2), bf), pltpu.VMEM(whole, bf),
            pltpu.VMEM((ROWS, 256), bf), pltpu.VMEM((ROWS, 128), fl),
            pltpu.VMEM((ROWS, ff), fl), pltpu.VMEM((ROWS, ff), fl), pltpu.VMEM((ROWS, 256 + 2 * HEADS), fl),
            pltpu.VMEM(whole, bf), pltpu.VMEM(whole, bf),
            *sum_set, *sum_set,
            *([pltpu.VMEM((ff, D), bf)] * 6),
            pltpu.VMEM((256 + 2 * HEADS, D), bf), pltpu.VMEM((128, D), bf),
            *([pltpu.VMEM((HEADS, HEAD, HEAD), fl)] * 2), *([pltpu.VMEM((128, 128), fl)] * 3),
            pltpu.SMEM((1,), jnp.int32), pltpu.VMEM((CHIPS, 2, BLK, 128), bf), pltpu.VMEM((CHIPS, 2, BLK, 128), bf),
            pltpu.VMEM((ROWS, 2 * HEADS), fl), pltpu.VMEM((2, 64, 128), bf), pltpu.VMEM((4, 64, 128), bf),
            pltpu.VMEM((2, 64, 128), bf), pltpu.VMEM((2, 2, 2, 64, 128), bf),
            dma((16,)), dma((7,)), dma((4, 2, 32)), dma((2, 2, 40)), dma((32,)), dma((2,)), dma((9,)), dma((12,)),
        ],
        compiler_params=pltpu.CompilerParams(
            collective_id=0, has_side_effects=True, vmem_limit_bytes=60_000_000
        ),
        name="layer",
    )(*arrays)


def store(out, state, out_hbm, state_hbm, out_vmem, state_vmem, sems):
    pieces = [(out, out_vmem, out_hbm)]
    for n in range(4):
        heads = pl.ds(4 * n, 4)
        pieces.append((state.at[heads], state_vmem.at[heads], state_hbm.at[heads]))
    reads = [pltpu.make_async_copy(a, b, sems.at[0, n]) for n, (a, b, _) in enumerate(pieces)]
    writes = [pltpu.make_async_copy(b, c, sems.at[1, n]) for n, (_, b, c) in enumerate(pieces)]
    for read in reads:
        read.start()
    for read, write in zip(reads, writes):
        read.wait()
        write.start()
    for write in writes:
        write.wait()


def stored(out, state):
    anywhere = pl.BlockSpec(memory_space=pl.ANY)
    return pl.pallas_call(
        store,
        out_shape=(jax.ShapeDtypeStruct(out.shape, out.dtype), jax.ShapeDtypeStruct(state.shape, state.dtype)),
        in_specs=[anywhere] * 2,
        out_specs=(anywhere,) * 2,
        scratch_shapes=[
            pltpu.VMEM(out.shape, out.dtype), pltpu.VMEM(state.shape, state.dtype), pltpu.SemaphoreType.DMA((2, 5)),
        ],
        compiler_params=pltpu.CompilerParams(vmem_limit_bytes=60_000_000),
        name="store",
    )(out, state)


def per_device(
    tokens,
    lengths,
    state,
    gain_first,
    first_gate,
    first_up,
    first_down,
    gain_mix,
    query_weight,
    key_weight,
    value_weight,
    gating_weight,
    write_weight,
    forget_weight,
    forget_rate,
    out_weight,
    gain_second,
    second_gate,
    second_up,
    second_down,
):
    out, new_state = run_layer(
        lengths, tokens.T, forget_rate[None, :], gain_first[None, :], gain_mix[None, :], gain_second[None, :],
        first_gate.T, first_up.T, first_down, second_gate.T, second_up.T, second_down,
        query_weight.T, key_weight.T, value_weight.T, gating_weight.T, out_weight.T,
        write_weight.T, forget_weight.T, state.reshape(HEADS, HEAD, HEAD),
    )
    out, new_state = stored(out, new_state)
    return out.T, new_state.reshape(state.shape)


def solution(mesh):
    in_specs = (
        P("dp", ("kv", "tp")),
        P(("dp", "kv", "tp")),
        P(("dp", "kv", "tp"), None, None, None),
        P(),
        P(None, "kv"),
        P(None, "kv"),
        P("kv", None),
        P(),
        P(None, ("kv", "tp")),
        P(None, ("kv", "tp")),
        P(None, ("kv", "tp")),
        P(None, ("kv", "tp")),
        P(),
        P(),
        P(),
        P(None, ("kv", "tp")),
        P(),
        P(None, "kv"),
        P(None, "kv"),
        P("kv", None),
    )
    out_specs = (P("dp", ("kv", "tp")), P(("dp", "kv", "tp"), None, None, None))
    return jax.shard_map(
        per_device, mesh=mesh, in_specs=in_specs, out_specs=out_specs, check_vma=False
    )
```

time: 168 us -> 127 us (0.76)
  Pallas kernels: 147 us -> 126 us
  local copies, waits for them, and re-layouts: 17.2 us -> 0 us
  other arithmetic: 2.05 us -> 0 us
    pallas_call x1 -> x2, Pallas kernels: 147 us -> 126 us  [the longest x1 124 us: run_layer(): pl.pallas_call(layer, out_shape=(jax.ShapeDtypeStruct((32, 512), bf), jax...]
    unnamed x36 -> x0, local copies, waits for them, and re-layouts: 12.3 us -> none
    pad x2 -> x0, local copies, waits for them, and re-layouts: 2.17 us -> none  [the longest x1 1.23 us: per_device(): rates = jnp.pad(forget_rate[None, :], ((0, 0), (HEADS, 128 - 2 * HEADS)))]
    concatenate x2 -> x0, other arithmetic: 1.97 us -> none  [the longest x1 1.96 us: per_device(): jnp.concatenate([query_weight, key_weight, value_weight, gating_weight],...]
where the time goes in v2:
time: 127 us
  Pallas kernels  126 us (99%)
  between operations  1.29 us (1%)
    pallas_call x1, Pallas kernels, run_layer(): pl.pallas_call(layer, out_shape=(jax.ShapeDtypeStruct((32, 512), bf), jax...  124 us

profile of v2, /device:TPU:1, one launch (start us, length us, event | category | flops | bytes accessed | tf_op | source)
XLA Modules:
  0.0 127.2 jit_solution(8419947312450536694)
XLA Ops:
  1.3 123.9 %layer.1 = (bf16[32,512]{1,0:T(8,128)(2,1)}, f32[16,128,128]{2,1,0:T(8,128)}) custom-call(s32[1]{0:T(128)S(6)} %copy.22.length, bf16[32,512]{1,0:T(8,128)(2,1)} %bitcast.31, f32[1,16]{1,0:T(1,128)} %bitcast.35, f32[1,2048]{1,0:T(1,128)} %bitcast.32, f32[1,2048]{1,0:T(1,128)} %bitcast.33, f32[1,2048]{1,0:T(1,128)} %bitcast.34, bf16[176,2048]{1,0:T(8,128)(2,1)} %bitcast.20, ...), custom_call_target="tpu_custom_call" | custom-call | tf_op jit(solution)/shard_map/layer/pallas_call | solution.py:570
  125.2 2.0 %store.1 = (bf16[32,512]{1,0:T(8,128)(2,1)}, f32[16,128,128]{2,1,0:T(8,128)}) custom-call(bf16[32,512]{1,0:T(8,128)(2,1)} %get-tuple-element.6.out, f32[16,128,128]{2,1,0:T(8,128)} %get-tuple-element.7.state), custom_call_target="tpu_custom_call" | custom-call | tf_op jit(solution)/shard_map/store/pallas_call | solution.py:618

commit v3 on v2

--- a/solution.py
+++ b/solution.py
@@ -52,20 +52,17 @@
 
 
 def children(half, dx, dz):
+    sign = 1 if half == 0 else -1
     dx, dz = dx % NX, wrapped(dz)
     if abs(dz) == 1:
         return []
     found = []
     if dx == 0:
+        found += [(sign, dz), (-sign, dz)]
         if dz == 0:
-            found += [(0, 4)]
-        if half == 0:
-            found += [(2, dz)]
-        found += [(-1, dz), (1, dz)]
-        if dz == 0:
-            found += [(0, 2), (0, -2), (0, 3), (0, -3), (0, 1), (0, -1)]
+            found += [(0, 2), (0, -2), (0, 3), (0, -3), (0, 4), (0, 1), (0, -1)]
     else:
-        if half == 1 and dx == NX - 1:
+        if dx == sign % NX:
             found += [(2, dz)]
         if dz == 0:
             found += [(dx, 1), (dx, -1)]
@@ -111,10 +108,11 @@
     pltpu.make_async_copy(ref, ref, sem).wait()
 
 
-def gather(torus, buf, send_sem, recv_sem, consume=None):
-    def pass_on(half, dx, dz):
+def gather(torus, buf, send_sem, recv_sem, consume=None, started=None):
+    def pass_on(half, dx, dz, only=None):
         source = torus.at(-dx, -dz)
-        for cx, cz in children(half, dx, dz):
+        targets = children(half, dx, dz)
+        for cx, cz in targets if only is None else targets[only : only + 1]:
             send(
                 buf.at[source, half],
                 buf.at[source, half],
@@ -127,8 +125,11 @@
         arrived(buf.at[torus.at(-dx, -dz), half], recv_sem.at[half, place(dx, dz)])
         pass_on(half, dx, dz)
 
-    for half in range(2):
-        pass_on(half, 0, 0)
+    for hop in range(len(children(0, 0, 0))):
+        for half in range(2):
+            pass_on(half, 0, 0, hop)
+    if started is not None:
+        started()
     for what, dz in GATHER_STEPS:
         if what == "column":
             take(0, 0, dz)
@@ -141,12 +142,13 @@
             take(0, 2, 0)
             take(1, 2, 0)
         elif what == "relay":
+            take(0, 1, dz)
             take(1, -1, dz)
         else:
             if abs(dz) == 1:
                 places = [(half, dx) for dx in (0, 1, -1, 2) for half in range(2)]
             elif dz != 0:
-                places = [(0, -1), (0, 1), (1, 1), (0, 2), (1, 2)]
+                places = [(0, -1), (1, 1), (0, 2), (1, 2)]
             else:
                 places = []
             for half, dx in places:
@@ -191,11 +193,11 @@
                     to_column(half, dx, dz, part.at[torus.at(-dx, -dz), half])
 
     def to_column(half, dx, dz, src):
-        if half == 1 and dx == 2:
-            post(src, relay.at[slot(dz)], half, slot(dz), torus.at(1, 0))
-        elif half == 0 or dx == 1:
-            n = {2: 2, 1: 0, -1: 1}[dx]
-            post(src, column.at[half, n, slot(dz)], half, (8, 16, 0)[n] + slot(dz), torus.at(-dx, 0))
+        sign = 1 if half == 0 else -1
+        if dx == 2:
+            post(src, relay.at[half, slot(dz)], half, slot(dz), torus.at(-sign, 0))
+        elif dx == -sign:
+            post(src, column.at[half, 0, slot(dz)], half, 8 + slot(dz), torus.at(sign, 0))
 
     def cross_row_step():
         for half in range(2):
@@ -203,20 +205,21 @@
                 for side in (1, -1):
                     n = z_slot(dx, side)
                     arrived(along_z.at[half, n], recv_sem.at[half, 32 + n])
-        for half, dx in ((1, 2), (0, 2), (0, 1), (0, -1), (1, 1)):
+        for half, dx in ((0, 2), (1, 2), (0, -1), (1, 1)):
             stage_row[half, dx % NX] = term(half, dx, 0).astype(BF16)
             to_column(half, dx, 0, stage_row.at[half, dx % NX])
 
-    def relay_step(dz):
-        arrived(relay.at[slot(dz)], recv_sem.at[1, slot(dz)])
-        total = term(1, -1, dz) + relay[slot(dz)].astype(F32)
-        stage_x[slot(dz)] = total.astype(BF16)
-        post(stage_x.at[slot(dz)], column.at[1, 1, slot(dz)], 1, 16 + slot(dz), torus.at(1, 0))
+    def relay_step(half, dz):
+        sign = 1 if half == 0 else -1
+        arrived(relay.at[half, slot(dz)], recv_sem.at[half, slot(dz)])
+        total = term(half, sign, dz) + relay[half, slot(dz)].astype(F32)
+        stage_x[half, slot(dz)] = total.astype(BF16)
+        post(stage_x.at[half, slot(dz)], column.at[half, 1, slot(dz)], half, 16 + slot(dz), torus.at(-sign, 0))
 
     def column_step(half, dz):
         total = term(half, 0, dz)
-        for n in range(3 - half):
-            arrived(column.at[half, n, slot(dz)], recv_sem.at[half, (8, 16, 0)[n] + slot(dz)])
+        for n in range(2):
+            arrived(column.at[half, n, slot(dz)], recv_sem.at[half, 8 + 8 * n + slot(dz)])
             total = total + column[half, n, slot(dz)].astype(F32)
         if dz == 0:
             sums[half] = total
@@ -230,7 +233,8 @@
         elif what == "cross_row":
             cross_row_step()
         elif what == "relay":
-            relay_step(dz)
+            relay_step(0, dz)
+            relay_step(1, dz)
         else:
             column_step(0, dz)
             column_step(1, dz)
@@ -266,7 +270,7 @@
 
 
 def half_step(torus, buf, gain_ref, gate_ref, up_ref, down_ref, weight_waits, scaled_ref, squares_ref,
-              acts, part, sum_refs, gather_sems, sum_sems, gathered=None):
+              acts, part, sum_refs, gather_sems, sum_sems, started=None, gathered=None):
     gate_act, up_act = acts
     squares_ref[...] = jnp.zeros_like(squares_ref)
     gate_act[...] = jnp.zeros_like(gate_act)
@@ -282,7 +286,7 @@
         up_act[...] += dot_nt(scaled, up_ref[:, channels])
 
     with jax.named_scope("gather"):
-        gather(torus, buf, *gather_sems, consume)
+        gather(torus, buf, *gather_sems, consume, started)
     if gathered is not None:
         gathered()
     with jax.named_scope("units"):
@@ -308,40 +312,47 @@
     return jnp.concatenate(parts, axis=0)
 
 
-def delta(owned, write_pre, forget_pre, rates, live, state, update_refs):
-    query, key, value, gating = owned
+def decays(write_pre, forget_pre, rates, live):
     live_heads = live[:, :HEADS]
     write = spread(jax.nn.sigmoid(write_pre) * live_heads)
     forget = spread(-jnp.exp(rates) * jax.nn.softplus(forget_pre) * live_heads)
+    row = lax.broadcasted_iota(jnp.int32, (128, 128), 0)
+    col = lax.broadcasted_iota(jnp.int32, (128, 128), 1)
+    causal = ((row >> 3) == (col >> 3)) & (col <= row)
+    cumulative = jnp.dot(
+        jnp.where(causal, 1.0, 0.0), forget, precision=HIGH, preferred_element_type=F32
+    )
+    decay = jnp.where(causal, jnp.exp(jnp.minimum(cumulative - cumulative.T, 0.0)), 0.0)
+    by_head = cumulative.reshape(HEADS, BLK, 128)
+    last = by_head[:, BLK - 1 : BLK, :]
+    fading = jnp.exp(last - by_head).reshape(128, 128)
+    kept = jnp.broadcast_to(jnp.exp(last), (HEADS, BLK, 128)).reshape(128, 128)
+    return write, jnp.exp(cumulative), decay, fading, kept
+
+
+def delta(owned, decays_ref, live, state, update_refs):
+    query, key, value, gating = owned
+    write, growth, decay = decays_ref[0], decays_ref[1], decays_ref[2]
     query_unit = query * lax.rsqrt(jnp.sum(query * query, axis=1, keepdims=True) + EPSILON)
     query_unit = query_unit / math.sqrt(HEAD)
     key_unit = key * lax.rsqrt(jnp.sum(key * key, axis=1, keepdims=True) + EPSILON)
     row = lax.broadcasted_iota(jnp.int32, (128, 128), 0)
     col = lax.broadcasted_iota(jnp.int32, (128, 128), 1)
-    same = (row >> 3) == (col >> 3)
-    causal = same & (col <= row)
-    strict = same & (col < row)
+    strict = col < row
     identity = jnp.where(row == col, 1.0, 0.0)
 
     def dot(a, b):
         return jnp.dot(a, b, precision=HIGH, preferred_element_type=F32)
 
-    cumulative = dot(jnp.where(causal, 1.0, 0.0), forget)
-    decay = jnp.where(causal, jnp.exp(jnp.minimum(cumulative - cumulative.T, 0.0)), 0.0)
     strict_part = jnp.where(strict, write * decay * dot_nt(key_unit, key_unit, HIGH), 0.0)
     squared = dot(strict_part, strict_part)
     fourth = dot(squared, squared)
     inverse = dot(dot(identity - strict_part, identity + squared), identity + fourth)
-    growth = jnp.exp(cumulative)
     target = dot(inverse, write * value)
     key_mix = dot(inverse, write * growth * key_unit)
     scores = dot_nt(query_unit, key_unit, HIGH) * decay
     grown = query_unit * growth
-    by_head = cumulative.reshape(HEADS, BLK, 128)
-    last = by_head[:, BLK - 1 : BLK, :]
-    fading = jnp.exp(last - by_head).reshape(128, 128)
-    faded = key_unit * fading
-    kept = jnp.exp(last)
+    faded = key_unit * decays_ref[3]
     updates, reads = [], []
     for h in range(HEADS):
         rows = slice(8 * h, 8 * h + 8)
@@ -350,10 +361,9 @@
         updates.append(target[rows] - seen[:BLK])
         reads.append(seen[BLK:])
     update = jnp.concatenate(updates, axis=0)
-    faded_ref, update_ref, kept_ref = update_refs
+    faded_ref, update_ref, _ = update_refs
     faded_ref[...] = faded
     update_ref[...] = update
-    kept_ref[...] = jnp.broadcast_to(kept, (HEADS, BLK, 128)).reshape(128, 128)
     attend = jnp.concatenate(reads, axis=0) + dot(scores, update)
     normed = attend * lax.rsqrt(jnp.mean(attend * attend, axis=1, keepdims=True) + EPSILON)
     return normed * jax.nn.silu(gating) * jnp.concatenate([live] * HEADS, axis=0)
@@ -366,12 +376,12 @@
     buf_a, buf_c, buf_m, buf_g, scaled, squares, gate_act, up_act, project, part1, part2,
     relay1, column1, final1, along1, stage_x1, stage_z1, stage_row1,
     relay2, column2, final2, along2, stage_x2, stage_z2, stage_row2,
-    v_gate1, v_up1, v_down1, v_gate2, v_up2, v_down2, v_all, v_out, v_state, v_fresh, faded_s, update_s, kept_s,
-    s_length, outgoing, incoming, gates, tok, tok_in, last_stage, last_in,
+    v_gate1, v_up1, v_down1, v_gate2, v_up2, v_down2, v_all, v_out, v_state, v_fresh, faded_s, update_s, decays_s,
+    v_tokens, v_rates, v_gains, s_length, outgoing, incoming, gates, tok, tok_in, last_stage, last_in,
     local_sem, send_sem, recv_ag, recv_rs, recv_x, pair_sem, quad_send, quad_recv,
 ):
     torus = Torus()
-    update_refs = (faded_s, update_s, kept_s)
+    update_refs = (faded_s, update_s, decays_s.at[4])
 
     def own_columns(t):
         return pl.multiple_of(128 * t, 128)
@@ -390,7 +400,7 @@
 
     with jax.named_scope("entry"):
         barrier = pltpu.get_barrier_semaphore()
-        near = [{"kv": torus.at(dx, 0)} for dx in (1, -1, 2)]
+        near = [{"kv": torus.at(dx, 0)} for dx in (1, -1)]
         near += [{"kv": torus.at(0, dz)} for dz in (1, -1, 2, -2, 3, -3, 4)]
         near += [{"tp": other}, {"kv": twin, "tp": other}]
         for target in near:
@@ -398,6 +408,7 @@
         loads = {}
         for n, (name, src, dst) in enumerate(
             [
+                ("tokens", tokens, v_tokens), ("gain1", gain_first, v_gains.at[0]),
                 ("gate1", gate1, v_gate1), ("up1", up1, v_up1), ("down1", down1, v_down1),
                 ("query", query, v_all.at[pl.ds(own_columns(tp), 32)]),
                 ("key", key, v_all.at[pl.ds(own_columns(tp) + 32, 32)]),
@@ -406,13 +417,16 @@
                 ("out", outw, v_out.at[own_out]),
                 ("write", writew, v_all.at[256:272]), ("forget", forgetw, v_all.at[272:288]),
                 ("state", state, v_state),
-                ("length", length, s_length), ("gate2", gate2, v_gate2), ("up2", up2, v_up2), ("down2", down2, v_down2),
+                ("length", length, s_length), ("rates", rates, v_rates),
+                ("gain_mix", gain_mix, v_gains.at[1]), ("gain2", gain_second, v_gains.at[2]),
+                ("gate2", gate2, v_gate2), ("up2", up2, v_up2), ("down2", down2, v_down2),
             ]
         ):
             loads[name] = pltpu.make_async_copy(src, dst, local_sem.at[n])
             loads[name].start()
 
-        values = tokens[...].astype(F32)
+        loads["tokens"].wait()
+        values = v_tokens[...].astype(F32)
         values = jnp.concatenate([values[:, 128 * q : 128 * q + 128] for q in range(4)], axis=0).T
         values = values.reshape(8, 2, BLK, 128)
         for parity in range(2):
@@ -430,32 +444,35 @@
             buf_a[kv, half] = jnp.where(odd == 0, tiles[half], tiles[2 + half]).astype(BF16)
     mine = v_all.at[pl.ds(own_columns(tp), 128)]
 
+    def share_out():
+        loads["out"].wait()
+        send(v_out.at[own_out], v_out.at[own_out], quad_send.at[4], quad_recv.at[4 + seat], {"kv": twin})
+
     def share_projections():
         for name in ("query", "key", "value", "gating"):
             loads[name].wait()
-        loads["out"].wait()
-        for n, (target, _) in enumerate(quad[:2]):
-            send(v_out.at[own_out], v_out.at[own_out], quad_send.at[3 + n], quad_recv.at[4 + seat], target)
+        send(v_out.at[own_out], v_out.at[own_out], quad_send.at[3], quad_recv.at[4 + seat], {"tp": other})
         send(mine, mine, pair_sem.at[0], pair_sem.at[1], {"tp": other})
 
     sums = half_step(
-        torus, buf_a, gain_first, v_gate1, v_up1, v_down1,
-        [loads["gate1"].wait, loads["up1"].wait, loads["down1"].wait],
+        torus, buf_a, v_gains.at[0], v_gate1, v_up1, v_down1,
+        [loads["gain1"].wait, loads["gate1"].wait, loads["up1"].wait, loads["down1"].wait],
         scaled, squares, (gate_act, up_act), part1,
         (relay1, column1, final1, along1, stage_x1, stage_z1, stage_row1),
-        (send_sem.at[0], recv_ag.at[0]), (send_sem.at[1], recv_rs.at[0]), share_projections,
+        (send_sem.at[0], recv_ag.at[0]), (send_sem.at[1], recv_rs.at[0]), share_out, share_projections,
     )
     for half in range(2):
         buf_c[kv, half] = (buf_a[kv, half].astype(F32) + 0.5 * sums[half]).astype(BF16)
 
     arrived(v_all.at[pl.ds(own_columns(other), 128)], pair_sem.at[1])
     loads["write"].wait()
+    loads["gain_mix"].wait()
     loads["forget"].wait()
     squares[...] = jnp.zeros_like(squares)
     project[...] = jnp.zeros_like(project)
 
     def consume(zt):
-        unpack_row(buf_c, gain_mix, scaled, squares, zt)
+        unpack_row(buf_c, v_gains.at[1], scaled, squares, zt)
         channels = pl.ds(pl.multiple_of(zt * 256, 256), 256)
         project[...] += dot_nt(scaled[...], v_all[:, channels])
 
@@ -477,6 +494,10 @@
         position = lax.broadcasted_iota(jnp.int32, (BLK, 128), 0)
         live = jnp.where(position < s_length[0], 1.0, 0.0)
         loads["state"].wait()
+        loads["rates"].wait()
+        gates_in = gates[own_rows, :]
+        for n, value in enumerate(decays(gates_in[:, :HEADS], gates_in[:, HEADS:], v_rates[...], live)):
+            decays_s[n] = value
         for d in range(1, CHIPS):
             arrived(incoming.at[lax.rem(kv + CHIPS - d, CHIPS)], recv_x.at[d])
     twin_seat = quad[1][1]
@@ -484,8 +505,7 @@
     with jax.named_scope("delta"):
         tiles = incoming[...].astype(F32).reshape(HEADS, 4, BLK, 128)
         owned = lanes_swapped([tiles[:, j].reshape(128, 128) for j in range(4)])
-        gates_in = gates[own_rows, :]
-        mixed = delta(owned, gates_in[:, :HEADS], gates_in[:, HEADS:], rates[...], live, v_state, update_refs)
+        mixed = delta(owned, decays_s, live, v_state, update_refs)
         for h in range(HEADS):
             lanes = slice(128 * (h % 8), 128 * (h % 8) + 128)
             buf_m[kv, h // 8, :, lanes] = mixed[8 * h : 8 * h + 8].astype(BF16)
@@ -500,7 +520,7 @@
 
     with jax.named_scope("gather_m"):
         gather(torus, buf_m, send_sem.at[4], recv_ag.at[2], renew_two)
-    save = pltpu.make_async_copy(v_fresh, new_state, local_sem.at[15])
+    save = pltpu.make_async_copy(v_fresh, new_state, local_sem.at[20])
     save.start()
     with jax.named_scope("out_product"):
         for place_at in (quad[0][1], quad[2][1]):
@@ -516,8 +536,8 @@
             buf_g[kv, half] = (buf_c[kv, half].astype(F32) + mixed_sum[rows]).astype(BF16)
 
     sums = half_step(
-        torus, buf_g, gain_second, v_gate2, v_up2, v_down2,
-        [loads["gate2"].wait, loads["up2"].wait, loads["down2"].wait],
+        torus, buf_g, v_gains.at[2], v_gate2, v_up2, v_down2,
+        [loads["gain2"].wait, loads["gate2"].wait, loads["up2"].wait, loads["down2"].wait],
         scaled, squares, (gate_act, up_act), part2,
         (relay2, column2, final2, along2, stage_x2, stage_z2, stage_row2),
         (send_sem.at[5], recv_ag.at[3]), (send_sem.at[6], recv_rs.at[1]),
@@ -564,8 +584,8 @@
     ff = 176
     eight = (8, 64, 128)
     sum_set = [
-        pltpu.VMEM(eight, bf), pltpu.VMEM((2, 3, *eight), bf), pltpu.VMEM((2, *eight), bf), pltpu.VMEM((2, *eight), bf),
-        pltpu.VMEM(eight, bf), pltpu.VMEM((2, *eight), bf), pltpu.VMEM((2, 4, 64, 128), bf),
+        pltpu.VMEM((2, *eight), bf), pltpu.VMEM((2, 2, *eight), bf), pltpu.VMEM((2, *eight), bf), pltpu.VMEM((2, *eight), bf),
+        pltpu.VMEM((2, *eight), bf), pltpu.VMEM((2, *eight), bf), pltpu.VMEM((2, 4, 64, 128), bf),
     ]
     return pl.pallas_call(
         layer,
@@ -573,7 +593,7 @@
             jax.ShapeDtypeStruct((32, 512), bf),
             jax.ShapeDtypeStruct((HEADS, HEAD, HEAD), fl),
         ),
-        in_specs=[in_hbm] + [in_vmem] * 5 + [in_hbm] * 14,
+        in_specs=[pl.BlockSpec(memory_space=pltpu.HBM)] + [in_hbm] * 19,
         out_specs=(in_vmem, in_hbm),
         scratch_shapes=[
             pltpu.VMEM(whole, bf), pltpu.VMEM(whole, bf),
@@ -584,11 +604,12 @@
             *sum_set, *sum_set,
             *([pltpu.VMEM((ff, D), bf)] * 6),
             pltpu.VMEM((256 + 2 * HEADS, D), bf), pltpu.VMEM((128, D), bf),
-            *([pltpu.VMEM((HEADS, HEAD, HEAD), fl)] * 2), *([pltpu.VMEM((128, 128), fl)] * 3),
+            *([pltpu.VMEM((HEADS, HEAD, HEAD), fl)] * 2), *([pltpu.VMEM((128, 128), fl)] * 2), pltpu.VMEM((5, 128, 128), fl),
+            pltpu.VMEM((32, 512), bf), pltpu.VMEM((1, HEADS), fl), pltpu.VMEM((3, 1, D), fl),
             pltpu.SMEM((1,), jnp.int32), pltpu.VMEM((CHIPS, 2, BLK, 128), bf), pltpu.VMEM((CHIPS, 2, BLK, 128), bf),
             pltpu.VMEM((ROWS, 2 * HEADS), fl), pltpu.VMEM((2, 64, 128), bf), pltpu.VMEM((4, 64, 128), bf),
             pltpu.VMEM((2, 64, 128), bf), pltpu.VMEM((2, 2, 2, 64, 128), bf),
-            dma((16,)), dma((7,)), dma((4, 2, 32)), dma((2, 2, 40)), dma((32,)), dma((2,)), dma((9,)), dma((12,)),
+            dma((21,)), dma((7,)), dma((4, 2, 32)), dma((2, 2, 40)), dma((32,)), dma((2,)), dma((9,)), dma((12,)),
         ],
         compiler_params=pltpu.CompilerParams(
             collective_id=0, has_side_effects=True, vmem_limit_bytes=60_000_000

time: 127 us -> 124 us (0.976)
  Pallas kernels: 126 us -> 122 us
    pallas_call x1, Pallas kernels: 124 us -> 120 us  [run_layer(): pl.pallas_call(layer, out_shape=(jax.ShapeDtypeStruct((32, 512), bf), jax...]
where the time goes in v3:
time: 124 us
  Pallas kernels  122 us (98%)
  between operations  1.29 us (1%)
    pallas_call x1, Pallas kernels, run_layer(): pl.pallas_call(layer, out_shape=(jax.ShapeDtypeStruct((32, 512), bf), jax...  120 us

profile of v3, /device:TPU:1, one launch (start us, length us, event | category | flops | bytes accessed | tf_op | source)
XLA Modules:
  0.0 123.7 jit_solution(13267903567021289951)
XLA Ops:
  1.3 120.4 %layer.1 = (bf16[32,512]{1,0:T(8,128)(2,1)}, f32[16,128,128]{2,1,0:T(8,128)}) custom-call(s32[1]{0:T(128)S(6)} %copy.22.length, bf16[32,512]{1,0:T(8,128)(2,1)} %bitcast.31, f32[1,16]{1,0:T(1,128)} %bitcast.35, f32[1,2048]{1,0:T(1,128)} %bitcast.32, f32[1,2048]{1,0:T(1,128)} %bitcast.33, f32[1,2048]{1,0:T(1,128)} %bitcast.34, bf16[176,2048]{1,0:T(8,128)(2,1)} %bitcast.20, ...), custom_call_target="tpu_custom_call" | custom-call | tf_op jit(solution)/shard_map/layer/pallas_call | solution.py:590
  121.7 2.0 %store.1 = (bf16[32,512]{1,0:T(8,128)(2,1)}, f32[16,128,128]{2,1,0:T(8,128)}) custom-call(bf16[32,512]{1,0:T(8,128)(2,1)} %get-tuple-element.6.out, f32[16,128,128]{2,1,0:T(8,128)} %get-tuple-element.7.state), custom_call_target="tpu_custom_call" | custom-call | tf_op jit(solution)/shard_map/store/pallas_call | solution.py:639

commit v4 on v3

--- a/solution.py
+++ b/solution.py
@@ -344,13 +344,14 @@
     def dot(a, b):
         return jnp.dot(a, b, precision=HIGH, preferred_element_type=F32)
 
-    strict_part = jnp.where(strict, write * decay * dot_nt(key_unit, key_unit, HIGH), 0.0)
+    products = dot_nt(jnp.concatenate([key_unit, query_unit], axis=0), key_unit, HIGH)
+    strict_part = jnp.where(strict, write * decay * products[:128], 0.0)
     squared = dot(strict_part, strict_part)
     fourth = dot(squared, squared)
     inverse = dot(dot(identity - strict_part, identity + squared), identity + fourth)
-    target = dot(inverse, write * value)
-    key_mix = dot(inverse, write * growth * key_unit)
-    scores = dot_nt(query_unit, key_unit, HIGH) * decay
+    solved = dot(inverse, jnp.concatenate([write * value, write * growth * key_unit], axis=1))
+    target, key_mix = solved[:, :128], solved[:, 128:]
+    scores = products[128:] * decay
     grown = query_unit * growth
     faded = key_unit * decays_ref[3]
     updates, reads = [], []
@@ -485,9 +486,10 @@
             outgoing[:, t] = product.reshape(CHIPS, BLK, 128).astype(BF16)
         gates[...] = project[:, 256:] * mix_scale
     with jax.named_scope("exchange"):
-        for d in range(1, CHIPS):
-            peer = lax.rem(kv + d, CHIPS)
-            send(outgoing.at[peer], incoming.at[kv], send_sem.at[3], recv_x.at[d], {"kv": peer})
+        offsets = [(dx, dz) for dz in (4, 3, -3, 2, -2, 1, -1, 0) for dx in (2, 1, -1, 0)][:-1]
+        for dx, dz in offsets:
+            peer = torus.at(dx, dz)
+            send(outgoing.at[peer], incoming.at[kv], send_sem.at[3], recv_x.at[place(dx, dz)], {"kv": peer})
         incoming[kv] = outgoing[kv]
         own_rows = pl.ds(pl.multiple_of(kv * BLK, BLK), BLK)
         loads["length"].wait()
@@ -498,8 +500,8 @@
         gates_in = gates[own_rows, :]
         for n, value in enumerate(decays(gates_in[:, :HEADS], gates_in[:, HEADS:], v_rates[...], live)):
             decays_s[n] = value
-        for d in range(1, CHIPS):
-            arrived(incoming.at[lax.rem(kv + CHIPS - d, CHIPS)], recv_x.at[d])
+        for dx, dz in offsets:
+            arrived(incoming.at[torus.at(-dx, -dz)], recv_x.at[place(dx, dz)])
     twin_seat = quad[1][1]
     twin_out = v_out.at[pl.ds(pl.multiple_of(32 * twin_seat, 32), 32)]
     with jax.named_scope("delta"):

time: 124 us -> 123 us (level)
  no operation moved by 1% of the time
where the time goes in v4:
time: 123 us
  Pallas kernels  122 us (99%)
  between operations  1.29 us (1%)
    pallas_call x1, Pallas kernels, run_layer(): pl.pallas_call(layer, out_shape=(jax.ShapeDtypeStruct((32, 512), bf), jax...  120 us

profile of v4, /device:TPU:1, one launch (start us, length us, event | category | flops | bytes accessed | tf_op | source)
XLA Modules:
  0.0 123.1 jit_solution(4250809830061313221)
XLA Ops:
  1.3 119.7 %layer.1 = (bf16[32,512]{1,0:T(8,128)(2,1)}, f32[16,128,128]{2,1,0:T(8,128)}) custom-call(s32[1]{0:T(128)S(6)} %copy.22.length, bf16[32,512]{1,0:T(8,128)(2,1)} %bitcast.31, f32[1,16]{1,0:T(1,128)} %bitcast.35, f32[1,2048]{1,0:T(1,128)} %bitcast.32, f32[1,2048]{1,0:T(1,128)} %bitcast.33, f32[1,2048]{1,0:T(1,128)} %bitcast.34, bf16[176,2048]{1,0:T(8,128)(2,1)} %bitcast.20, ...), custom_call_target="tpu_custom_call" | custom-call | tf_op jit(solution)/shard_map/layer/pallas_call | solution.py:592
  121.0 2.0 %store.1 = (bf16[32,512]{1,0:T(8,128)(2,1)}, f32[16,128,128]{2,1,0:T(8,128)}) custom-call(bf16[32,512]{1,0:T(8,128)(2,1)} %get-tuple-element.6.out, f32[16,128,128]{2,1,0:T(8,128)} %get-tuple-element.7.state), custom_call_target="tpu_custom_call" | custom-call | tf_op jit(solution)/shard_map/store/pallas_call | solution.py:641
